TPU v7x, 32 devices: a whole 2x2x4 slice. The times are simulated.
32 devices in a mesh: sp: 16 (over z, y, x), tp: 2 (over core).
Axes of the slice: x: 2, y: 2, z: 4, core: 2. Of those that a mesh axis runs over, the one named last changes fastest.
Arguments:
- acceptor_signal: bfloat16 [2048, 1024], P('sp', 'tp'), may hold values from -6 to 6
- address_entries: bfloat16 [2048, 1024], P('sp', 'tp'), may hold values from -6 to 6
- payload_entries: bfloat16 [2048, 1024], P('sp', 'tp'), may hold values from -6 to 6
- fading_logits: float32 [2048, 1024], P('sp', 'tp'), may hold values from -12 to -2
- learning_rate_logits: float32 [2048, 1024], P('sp', 'tp'), may hold values from -10 to 4
- exit_switch_entries: bfloat16 [2048, 1024], P('sp', 'tp'), may hold values from -6 to 6
- extra_reward_weights: float32 [1024], P('tp'), may hold values from -0.3 to 0.3
- subspace_rescale_weights: float32 [1024], P('tp'), may hold values from 0.1 to 1.9
- timemix_exit_weights: bfloat16 [1024, 2048], P('tp'), may hold values from -0.1875 to 0.1875
- skip_stream_arriving: bfloat16 [2048, 2048], P(('sp', 'tp')), may hold values from -6 to 6
- pointwise_block_scaling: float32 [2048], replicated, may hold values from 0.1 to 1.9
- switch_projection: bfloat16 [2048, 5632], P('sp', 'tp'), may hold values from -0.125 to 0.125
- widening_projection: bfloat16 [2048, 5632], P('sp', 'tp'), may hold values from -0.125 to 0.125
- switch_filter_coefficients: float32 [3, 5632], P(None, 'tp'), may hold values from -3.5 to 3.5
- narrowing_projection: bfloat16 [5632, 2048], P('tp', 'sp'), may hold values from -0.078125 to 0.078125
Outputs:
- layer_out: bfloat16 [2048, 2048], P(('sp', 'tp'))
All inputs are finite; a program needn't handle non-finite values.
Results may differ from a plain program's by a relative error of at most 0.019.
Values may be sent and summed in bfloat16 or wider, within the bound.
A program may use at most 128 MiB of HBM per device.

v0:
```python
import jax
import jax.numpy as jnp
from jax import lax
from jax.sharding import PartitionSpec as P

SUBSPACE_WIDTH = 64
SPAN = 16


group_eps = 0.00064
norm_eps = 1e-06
highest = lax.Precision.HIGHEST


def carried_in(shard, axis, join, neutral):
    place = lax.axis_index(axis)
    gathered = jax.tree.map(
        lambda a, kind: lax.all_gather(a.astype(kind), axis), shard, (jnp.bfloat16, jnp.bfloat16)
    )
    state = jax.tree.map(lambda a, e: jnp.zeros_like(a) + jnp.asarray(e, a.dtype), shard, neutral)

    def one(lap, state):
        return join(
            state,
            jax.tree.map(
                lambda a, own: lax.dynamic_index_in_dim(a, lap, 0, False).astype(own.dtype),
                gathered,
                shard,
            ),
        )

    return lax.fori_loop(0, place, one, state)


def shifted(block, axis, distance):
    devices = range(lax.axis_size(axis))
    route = [(i - distance, i) for i in devices if i - distance in devices]
    return lax.ppermute(block, axis, route)


def by_heads(array):
    return array.astype(jnp.float32).reshape(array.shape[0], -1, SUBSPACE_WIDTH)


def mechanism_inputs(
    acceptor_signal, address_entries, payload_entries, fading_logits, learning_rate_logits
):
    acceptor_entries = by_heads(acceptor_signal)
    address_mapped = by_heads(address_entries)
    payload_mapped = by_heads(payload_entries)
    log_rate = -jax.nn.softplus(-fading_logits) - 0.5
    fading = by_heads(jnp.exp(-jnp.exp(log_rate)))
    erase_rate = by_heads(jax.nn.sigmoid(learning_rate_logits))
    length = jnp.sqrt(jnp.sum(address_mapped * address_mapped, axis=-1, keepdims=True))
    unit_key = address_mapped / jnp.maximum(length, 1.0)
    return (
        acceptor_entries,
        address_mapped,
        payload_mapped,
        fading,
        -unit_key,
        unit_key * erase_rate,
    )


def subspace_outcomes(
    acceptor_entries,
    address_mapped,
    payload_mapped,
    closing_memory,
    subspace_rescale_weights,
    extra_reward_weights,
    exit_switch_entries,
):
    centred = closing_memory - jnp.mean(closing_memory, axis=-1, keepdims=True)
    rescaled_arguments = centred * lax.rsqrt(
        jnp.mean(centred * centred, axis=-1, keepdims=True) + group_eps
    )
    scaling_fetch = subspace_rescale_weights.reshape(-1, SUBSPACE_WIDTH)
    extra_reward_fetch = extra_reward_weights.reshape(-1, SUBSPACE_WIDTH)
    present_extra_reward = (
        jnp.sum(acceptor_entries * address_mapped * extra_reward_fetch, axis=-1, keepdims=True)
        * payload_mapped
    )
    timemix_product = rescaled_arguments * scaling_fetch + present_extra_reward
    timemix_product = timemix_product.reshape(
        timemix_product.shape[0], -1
    ) * exit_switch_entries.astype(jnp.float32)
    return timemix_product.astype(jnp.bfloat16)


def compose(earlier, latter):
    mapping = jnp.einsum("...ij,...jk->...ik", earlier[0], latter[0], precision=highest)
    state = jnp.einsum("...ij,...jk->...ik", earlier[1], latter[0], precision=highest) + latter[1]
    return (mapping, state)


def span_step(carried, sublevel_arguments):
    state, mapping = carried
    acceptor_entries, address_mapped, payload_mapped, fading, erase_dir, erase_amt = (
        sublevel_arguments
    )
    along = jnp.einsum("bhij,bhj->bhi", state, erase_dir, precision=highest)
    map_along = jnp.einsum("bhij,bhj->bhi", mapping, erase_dir, precision=highest)
    state = (
        state * fading[:, :, None, :]
        + along[..., None] * erase_amt[:, :, None, :]
        + payload_mapped[..., None] * address_mapped[:, :, None, :]
    )
    mapping = mapping * fading[:, :, None, :] + map_along[..., None] * erase_amt[:, :, None, :]
    local_out = jnp.einsum("bhij,bhj->bhi", state, acceptor_entries, precision=highest)
    probe = jnp.einsum("bhij,bhj->bhi", mapping, acceptor_entries, precision=highest)
    return ((state, mapping), (local_out, probe))


def recurrence(sublevel_arguments):
    token_count, head_count = (sublevel_arguments[0].shape[0], sublevel_arguments[0].shape[1])
    blocks = token_count // SPAN

    def arrange(member):
        return jnp.moveaxis(member.reshape(blocks, SPAN, head_count, SUBSPACE_WIDTH), 1, 0)

    arranged = tuple((arrange(member) for member in sublevel_arguments))
    unit_map = jnp.eye(SUBSPACE_WIDTH, dtype=jnp.float32)
    zero_state = jnp.zeros((blocks, head_count, SUBSPACE_WIDTH, SUBSPACE_WIDTH), jnp.float32)
    start_maps = jnp.broadcast_to(unit_map, zero_state.shape)
    (block_states, block_maps), (local_out, probe) = lax.scan(
        span_step, (zero_state, start_maps), arranged
    )
    cum_maps, cum_states = lax.associative_scan(compose, (block_maps, block_states))
    head_unit = jnp.broadcast_to(unit_map, (head_count, SUBSPACE_WIDTH, SUBSPACE_WIDTH))
    head_zero = jnp.zeros((head_count, SUBSPACE_WIDTH, SUBSPACE_WIDTH), jnp.float32)
    _, incoming = carried_in((cum_maps[-1], cum_states[-1]), "sp", compose, (head_unit, head_zero))
    prior_maps = jnp.concatenate([head_unit[None], cum_maps[:-1]], axis=0)
    prior_states = jnp.concatenate([head_zero[None], cum_states[:-1]], axis=0)
    entry = jnp.einsum("hij,bhjk->bhik", incoming, prior_maps, precision=highest) + prior_states
    closing_memory = local_out + jnp.einsum("bhij,tbhj->tbhi", entry, probe, precision=highest)
    return jnp.moveaxis(closing_memory, 0, 1).reshape(token_count, head_count, SUBSPACE_WIDTH)


def body(
    acceptor_signal,
    address_entries,
    payload_entries,
    fading_logits,
    learning_rate_logits,
    exit_switch_entries,
    extra_reward_weights,
    subspace_rescale_weights,
    timemix_exit_weights,
    skip_stream_arriving,
    pointwise_block_scaling,
    switch_projection,
    widening_projection,
    switch_filter_coefficients,
    narrowing_projection,
):
    gate_full, up_full, down_full = (
        lax.all_gather(switch_projection, "sp", axis=0, tiled=True),
        lax.all_gather(widening_projection, "sp", axis=0, tiled=True),
        lax.all_gather(narrowing_projection, "sp", axis=1, tiled=True),
    )
    sublevel_arguments = mechanism_inputs(
        acceptor_signal, address_entries, payload_entries, fading_logits, learning_rate_logits
    )
    closing_memory = recurrence(sublevel_arguments)
    timemix_product = subspace_outcomes(
        sublevel_arguments[0],
        sublevel_arguments[1],
        sublevel_arguments[2],
        closing_memory,
        subspace_rescale_weights,
        extra_reward_weights,
        exit_switch_entries,
    )
    token_count = timemix_product.shape[0]
    picked = timemix_product
    attended = lax.psum_scatter(
        jnp.dot(picked, timemix_exit_weights, preferred_element_type=jnp.float32).astype(
            jnp.bfloat16
        ),
        "tp",
        scatter_dimension=0,
        tiled=True,
    ).astype(jnp.float32)
    hidden_res = skip_stream_arriving.astype(jnp.float32) + attended
    rescaled_arguments = (
        hidden_res
        * lax.rsqrt(jnp.mean(hidden_res * hidden_res, axis=-1, keepdims=True) + norm_eps)
        * pointwise_block_scaling
    )
    rescaled_arguments = rescaled_arguments.astype(jnp.bfloat16)
    all_rows = lax.all_gather(rescaled_arguments, "tp", axis=0, tiled=True)
    gate_acc = jnp.dot(all_rows, gate_full, preferred_element_type=jnp.float32)
    up_acc = jnp.dot(all_rows, up_full, preferred_element_type=jnp.float32)
    gate_pre = gate_acc.astype(jnp.bfloat16)
    up_part = up_acc.astype(jnp.bfloat16)
    taps = switch_filter_coefficients.shape[0]
    tail_rows = shifted(gate_pre[token_count - taps + 1 :], "sp", 1)
    extended = jnp.concatenate([tail_rows, gate_pre], axis=0).astype(jnp.float32)
    conv_out = jnp.zeros(gate_pre.shape, jnp.float32)
    for tap in range(taps):
        conv_out = conv_out + switch_filter_coefficients[tap] * extended[tap : tap + token_count]
    hidden = (jax.nn.silu(conv_out) * up_part.astype(jnp.float32)).astype(jnp.bfloat16)
    picked = hidden
    projected = lax.psum_scatter(
        jnp.dot(picked, down_full, preferred_element_type=jnp.float32).astype(jnp.bfloat16),
        "tp",
        scatter_dimension=0,
        tiled=True,
    ).astype(jnp.float32)
    return (hidden_res + projected).astype(jnp.bfloat16)


def solution(mesh):
    return jax.shard_map(
        body,
        mesh=mesh,
        in_specs=(
            P("sp", "tp"),
            P("sp", "tp"),
            P("sp", "tp"),
            P("sp", "tp"),
            P("sp", "tp"),
            P("sp", "tp"),
            P("tp"),
            P("tp"),
            P("tp", None),
            P(("sp", "tp"), None),
            P(),
            P("sp", "tp"),
            P("sp", "tp"),
            P(None, "tp"),
            P("tp", "sp"),
        ),
        out_specs=P(("sp", "tp"), None),
        check_vma=False,
    )
```

profile of v0, /device:TPU:0, one launch (start us, length us, event | category | flops | bytes accessed | tf_op | source)
XLA Modules:
  0.0 1192.7 jit_solution(1004884859613980477)
XLA Ops:
  23.3 418.0 %while.30 = (s32[]{:T(128)}, f32[8,8,64,64]{3,2,1,0:T(8,128)}, f32[8,8,64,64]{3,2,1,0:T(8,128)}, f32[16,8,8,64]{3,0,2,1:T(8,128)}, f32[16,8,8,64]{3,0,2,1:T(8,12...) while((s32[]{:T(128)}, f32[8,8,64,64]{3,2,1,0:T(8,128)}, ...), condition=%wide.region_2.3_spmd.clone, body=%wide.region_1.2_spmd.clone.sunk | while | flops 15204355 | bytes 25657612 | solution.py:127
  41.1 4.9 convolution_bitcast_fusion.9
  48.5 5.1 fusion.113
  67.3 4.9 convolution_bitcast_fusion.9
  74.8 5.1 fusion.113
  93.5 4.9 convolution_bitcast_fusion.9
  101.0 5.1 fusion.113
  119.7 4.9 convolution_bitcast_fusion.9
  127.2 5.1 fusion.113
  146.0 4.9 convolution_bitcast_fusion.9
  153.4 5.1 fusion.113
  172.2 4.9 convolution_bitcast_fusion.9
  179.7 5.1 fusion.113
  198.4 4.9 convolution_bitcast_fusion.9
  205.9 5.1 fusion.113
  224.6 4.9 convolution_bitcast_fusion.9
  232.1 5.1 fusion.113
  250.9 4.9 convolution_bitcast_fusion.9
  258.4 5.1 fusion.113
  277.1 4.9 convolution_bitcast_fusion.9
  284.6 5.1 fusion.113
  303.3 4.9 convolution_bitcast_fusion.9
  310.8 5.1 fusion.113
  329.6 4.9 convolution_bitcast_fusion.9
  337.1 5.1 fusion.113
  355.8 4.9 convolution_bitcast_fusion.9
  363.3 5.1 fusion.113
  382.1 4.9 convolution_bitcast_fusion.9
  389.6 5.1 fusion.113
  415.8 5.1 fusion.113
  452.4 9.2 pad.48
  463.5 9.2 pad.47
  478.5 16.6 %pad.50 = f32[8,8,64,64]{3,2,1,0:T(8,128)} pad(f32[4,8,64,64]{3,2,1,0:T(8,128)} %copy-done.6, f32[]{:T(128)} %constant.54.clone.1), padding=1_0_1x0_0_0x0_0_0x0_0_0 | pad | bytes 1572868 | tf_op jit(solution)/shard_map/pad | solution.py:130
  497.4 16.7 %pad.49 = f32[8,8,64,64]{3,2,1,0:T(8,128)} pad(f32[4,8,64,64]{3,2,1,0:T(8,128)} %pad_maximum_fusion.1, f32[]{:T(128)} %constant.54.clone.1), padding=0_1_1x0_0_0x0_0_0x0_0_0 | pad | bytes 1572868 | tf_op jit(solution)/shard_map/pad | solution.py:130
  518.8 5.9 pad.41
  525.8 5.9 pad.42
  533.4 11.1 pad.112
  546.2 16.6 %pad.67 = f32[7,8,64,64]{3,2,1,0:T(8,128)} pad(f32[4,8,64,64]{3,2,1,0:T(8,128)} %pad_maximum_fusion.1, f32[]{:T(128)} %constant.54.clone.1), padding=0_0_1x0_0_0x0_0_0x0_0_0 | pad | bytes 1441796 | tf_op jit(solution)/shard_map/slice | solution.py:135
  563.8 11.2 pad.44
  577.1 11.2 pad.43
  594.9 46.1 %all-gather.6.cloned.1.call-done = bf16[16,8,64,64]{3,2,1,0:T(8,128)(2,1)} async-done(((bf16[1,8,64,64]{3,2,1,0:T(8,128)(2,1)}), bf16[16,8,64,64]{3,2,1,0:T(8,128)(2,1)}) %all-gather.6.cloned.1.call-update) | async-done | bytes 1048592 | tf_op jit(solution)/shard_map/all_gather | solution.py:18
  654.4 39.6 %reduce-scatter.3.cloned.1.call-done = bf16[64,2048]{1,0:T(8,128)(2,1)} async-done(((bf16[128,2048]{1,0:T(8,128)(2,1)}), bf16[64,2048]{1,0:T(8,128)(2,1)}) %reduce-scatter.3.cloned.1.call-update) | async-done | bytes 262160 | tf_op jit(solution)/shard_map/reduce_scatter | solution.py:178
  698.4 140.8 %all-gather.10.cloned.1.call-done = bf16[2048,2816]{1,0:T(8,128)(2,1)} async-done(((bf16[128,2816]{1,0:T(8,128)(2,1)}), bf16[2048,2816]{1,0:T(8,128)(2,1)}) %all-gather.10.cloned.1.call-update) | async-done | bytes 11534352 | tf_op jit(solution)/shard_map/all_gather | solution.py:159
  839.1 6.0 convolution_convert_fusion.1
  851.0 130.4 %all-gather.12.cloned.1.call-done = bf16[2048,2816]{1,0:T(8,128)(2,1)} async-done(((bf16[128,2816]{1,0:T(8,128)(2,1)}), bf16[2048,2816]{1,0:T(8,128)(2,1)}) %all-gather.12.cloned.1.call-update) | async-done | bytes 11534352 | tf_op jit(solution)/shard_map/all_gather | solution.py:160
  981.4 182.8 %all-gather.14.cloned.1.call-done = bf16[2816,2048]{1,0:T(8,128)(2,1)} async-done(((bf16[2816,128]{1,0:T(8,128)(2,1)}), bf16[2816,2048]{1,0:T(8,128)(2,1)}) %all-gather.14.cloned.1.call-update) | async-done | bytes 11534352 | tf_op jit(solution)/shard_map/all_gather | solution.py:161
  1164.2 13.6 %convolution_convert_fusion.2 = bf16[128,2048]{1,0:T(8,128)(2,1)} fusion(bf16[2816,2048]{1,0:T(8,128)(2,1)} %all-gather.14.cloned.1.call-done, bf16[128,2048]{1,0:T(8,128)(2,1)S(1)} %all_gather.22, bf16[2048,2816]{1,0:T(8,128)(2,1)} %all-gather.12.cloned.1.call-done, f32[130,2816]{1,0:T(8,128)} %maximum_convert_fusion, f32[2816]{0:T(1024)S(1)} %get-tuple-element.188, ...), kind=kOutput, calls=%fused_computation.27 | convolution fusion | flops 2957737984 | bytes 28476416 | tf_op jit(solution)/shard_map/dot_general | solution.py:207
  1177.8 6.3 reduce-scatter.5.cloned.1.call-done
  (402 shorter events, 353.2 us)
Async XLA Ops:
  6.5 643.8 %copy-start = (bf16[512,2048]{1,0:T(8,128)(2,1)S(1)}, bf16[512,2048]{1,0:T(8,128)(2,1)}, u32[]{:S(2)}) copy-start(bf16[512,2048]{1,0:T(8,128)(2,1)} %param.27) | copy-start | bytes 6291460
  6.5 588.4 %all-gather.8.cloned.1.call-start = ((), (), s32[]{:S(2)}) async-start(), calls=%async_computation.3 | async-start | bytes 2228224 | tf_op jit(solution)/shard_map/all_gather | solution.py:18
  7.9 13.7 %copy-start.21 = (f32[64,64]{1,0:T(8,128)}, f32[64,64]{1,0:T(8,128)S(1)}, u32[]{:S(2)}) copy-start(f32[64,64]{1,0:T(8,128)S(1)} %fusion.61) | copy-start | bytes 49156
  12.0 9.6 copy-start.15
  24.1 8.3 copy-start.4
  48.5 5.1 copy-start.1
  48.5 10.0 copy-start.4
  74.8 5.1 copy-start.1
  74.8 10.0 copy-start.4
  101.0 5.1 copy-start.1
  101.0 10.0 copy-start.4
  127.2 5.1 copy-start.1
  127.2 10.0 copy-start.4
  153.4 5.1 copy-start.1
  153.4 10.0 copy-start.4
  179.6 5.1 copy-start.1
  179.6 10.0 copy-start.4
  205.9 5.1 copy-start.1
  205.9 10.0 copy-start.4
  232.1 5.1 copy-start.1
  232.1 10.0 copy-start.4
  258.3 5.1 copy-start.1
  258.3 10.0 copy-start.4
  284.6 5.1 copy-start.1
  284.6 10.0 copy-start.4
  310.8 5.1 copy-start.1
  310.8 10.0 copy-start.4
  337.1 5.1 copy-start.1
  337.1 10.0 copy-start.4
  363.3 5.1 copy-start.1
  363.3 10.0 copy-start.4
  389.5 10.0 copy-start.4
  415.8 10.0 copy-start.4
  450.7 10.9 slice-start
  478.5 16.6 %copy-start.17 = (f32[1,8,64,64]{3,2,1,0:T(8,128)S(1)}, f32[1,8,64,64]{3,2,1,0:T(8,128)}, u32[]{:S(2)}) copy-start(f32[1,8,64,64]{3,2,1,0:T(8,128)} %slice.129) | copy-start | bytes 393220
  515.8 125.2 %all-gather.6.cloned.1.call-start = ((), (), s32[]{:S(2)}) async-start(), calls=%async_computation.2 | async-start | bytes 2228224 | tf_op jit(solution)/shard_map/all_gather | solution.py:18
  546.1 147.8 %reduce-scatter.3.cloned.1.call-start = ((), (), s32[]{:S(2)}) async-start(), calls=%async_computation.4 | async-start | bytes 786432 | tf_op jit(solution)/shard_map/reduce_scatter | solution.py:178
  577.1 11.3 copy-start.26
  577.1 11.3 copy-start.16
  652.6 41.4 %copy-start.12 = (bf16[64,2048]{1,0:T(8,128)(2,1)S(1)}, bf16[64,2048]{1,0:T(8,128)(2,1)}, u32[]{:S(2)}) copy-start(bf16[64,2048]{1,0:T(8,128)(2,1)} %param.28) | copy-start | bytes 786436
  652.6 42.6 %copy-start.24 = (f32[2048]{0:T(1024)S(1)}, f32[2048]{0:T(1024)}, u32[]{:S(2)}) copy-start(f32[2048]{0:T(1024)} %param.29) | copy-start | bytes 24580
  652.6 186.6 %all-gather.10.cloned.1.call-start = ((), (), s32[]{:S(2)}) async-start(), calls=%async_computation.5 | async-start | bytes 12255232 | tf_op jit(solution)/shard_map/all_gather | solution.py:159
  653.2 328.2 %all-gather.12.cloned.1.call-start = ((), (), s32[]{:S(2)}) async-start(), calls=%async_computation.6 | async-start | bytes 12255232 | tf_op jit(solution)/shard_map/all_gather | solution.py:160
  653.7 510.5 %all-gather.14.cloned.1.call-start = ((), (), s32[]{:S(2)}) async-start(), calls=%async_computation.7 | async-start | bytes 12255232 | tf_op jit(solution)/shard_map/all_gather | solution.py:161
  654.3 529.8 %reduce-scatter.5.cloned.1.call-start = ((), (), s32[]{:S(2)}) async-start(), calls=%async_computation.8 | async-start | bytes 786432 | tf_op jit(solution)/shard_map/reduce_scatter | solution.py:206
  698.4 150.2 %copy-start.23 = (f32[3,2816]{1,0:T(4,128)S(1)}, f32[3,2816]{1,0:T(4,128)}, u32[]{:S(2)}) copy-start(f32[3,2816]{1,0:T(4,128)} %param.32) | copy-start | bytes 101380
  845.1 4.6 collective-permute-start
  1164.2 19.9 %copy-start.13 = (bf16[64,2048]{1,0:T(8,128)(2,1)S(1)}, bf16[64,2048]{1,0:T(8,128)(2,1)}, u32[]{:S(2)}) copy-start(bf16[64,2048]{1,0:T(8,128)(2,1)} %reduce-scatter.3.cloned.1.call-done) | copy-start | bytes 786436
  (48 other events, 146.9 us)
Sparse Core Ops, SparseCore 0:
  515.9 63.0 all-gather.7
  581.9 59.1 all-gather.5
  652.7 41.2 reduce-scatter.2
  696.6 142.5 all-gather.9
  841.7 139.5 all-gather.11
  983.9 180.2 all-gather.13
  1178.0 6.0 reduce-scatter.4
where the time goes:
time: 1210 us; the launch traced here: 1190 us
  waiting for transfers between devices  549 us (45%)
  matrix products  311 us (26%)
  local copies, waits for them, and re-layouts  248 us (20%)
  other arithmetic  64.1 us (5%)
  between operations  14.1 us (1%)
    all_gather x1, waiting for transfers between devices, body(): lax.all_gather(narrowing_projection, 'sp', axis=1, tiled=True)  183 us
    all_gather x1, waiting for transfers between devices, body(): lax.all_gather(switch_projection, 'sp', axis=0, tiled=True)  141 us
    all_gather x1, waiting for transfers between devices, body(): lax.all_gather(widening_projection, 'sp', axis=0, tiled=True)  130 us
    pad x8, local copies, waits for them, and re-layouts, recurrence(): lax.associative_scan(compose, (block_maps, block_states))  86 us
    dot_general x16, matrix products, span_step(): along = jnp.einsum('bhij,bhj->bhi', state, erase_dir, precision=highest)  79.9 us
    dot_general x16, matrix products, span_step(): jnp.einsum('bhij,bhj->bhi', state, acceptor_entries, precision=highest)  79 us
    dynamic_update_slice x32, local copies, waits for them, and re-layouts, recurrence(): lax.scan(span_step, (zero_state, start_maps), arranged)  57 us
    dot_general x16, matrix products, span_step(): jnp.einsum('bhij,bhj->bhi', mapping, erase_dir, precision=highest)  53.9 us
  transfers between devices with their start and end apart: 8, of which 7 were waited for; matrix products, arithmetic and copies ran while one was open for 7% of the time, Pallas kernels for 0%

commit v1 on v0

v1 whole, which is shorter than its diff:
```python
import functools

import jax
import jax.numpy as jnp
from jax import lax
from jax.experimental import pallas as pl
from jax.experimental.pallas import tpu as pltpu
from jax.sharding import Mesh, PartitionSpec as P

WIDTH = 64
GROUP = 4
group_eps = 0.00064
norm_eps = 1e-06
f32, bf16 = jnp.float32, jnp.bfloat16
NN, NT, TN = ((1,), (0,)), ((1,), (1,)), ((0,), (0,))


def split(a):
    high = a.astype(bf16)
    return high, (a - high.astype(f32)).astype(bf16)


def dot(a, b, dims=NN):
    return lax.dot_general(a, b, (dims, ((), ())), preferred_element_type=f32)


def dot3(a, b, dims=NN):
    (ah, al), (bh, bl) = a, b
    return dot(ah, bh, dims) + (dot(ah, bl, dims) + dot(al, bh, dims))


def chunk_kernel(r_ref, k_ref, v_ref, x_ref, l_ref, q_ref, o_ref, m_ref):
    tokens, lanes = r_ref.shape
    row = lax.broadcasted_iota(jnp.int32, (tokens, tokens), 0)
    col = lax.broadcasted_iota(jnp.int32, (tokens, tokens), 1)
    log_decay = -jax.nn.sigmoid(x_ref[...]) * jnp.exp(jnp.asarray(-0.5, f32))
    ones = (row >= col).astype(bf16)
    d0, rest = split(log_decay)[0], log_decay
    rest = log_decay - d0.astype(f32)
    d1, d2 = split(rest)
    running = dot(ones, d0) + (dot(ones, d1) + dot(ones, d2))
    decay = jnp.exp(running)
    before = jnp.exp(running - log_decay)
    inverse = jnp.exp(-running)
    rate = jax.nn.sigmoid(l_ref[...])
    r_all, k_all, v_all = (a[...].astype(f32) for a in (r_ref, k_ref, v_ref))
    k_hat_all = k_all * inverse
    r_hat_all = r_all * decay
    for head in range(lanes // WIDTH):
        cut = slice(head * WIDTH, (head + 1) * WIDTH)
        k = k_all[:, cut]
        length = jnp.sqrt(jnp.sum(k * k, axis=-1, keepdims=True))
        unit = k / jnp.maximum(length, 1.0)
        a_hat = -unit * before[:, cut]
        b_hat = unit * rate[:, cut] * inverse[:, cut]
        k_hat, r_hat = k_hat_all[:, cut], r_hat_all[:, cut]
        v = v_ref[:, cut]
        bk = split(jnp.concatenate([b_hat, k_hat], axis=0))
        both = dot3(split(jnp.concatenate([a_hat, r_hat], axis=0)), bk, NT)
        erase = jnp.where(row > col, both[:tokens, :tokens], 0.0)
        write = jnp.where(row > col, both[:tokens, tokens:], 0.0)
        out_erase = jnp.where(row >= col, both[tokens:, :tokens], 0.0)
        out_write = jnp.where(row >= col, both[tokens:, tokens:], 0.0)
        solved = (row == col).astype(f32)
        block = 1
        while block < tokens:
            off = (row // block == col // block + 1) & (row // (2 * block) == col // (2 * block))
            part = jnp.where(off, erase, 0.0)
            if block == 1:
                solved = solved + part
            else:
                pieces = split(solved)
                solved = solved + dot3(split(dot3(pieces, split(part))), pieces)
            block *= 2
        wh, wl = split(write)
        seen = jnp.concatenate([a_hat, dot(wh, v) + dot(wl, v)], axis=1)
        kept = dot3(split(solved), split(seen))
        kept_pieces = split(kept)
        oh, ol = split(out_write)
        out = dot3(split(out_erase), kept_pieces) + jnp.concatenate(
            [r_hat, dot(oh, v) + dot(ol, v)], axis=1
        )
        q_ref[:, cut] = out[:, :WIDTH]
        o_ref[:, cut] = out[:, WIDTH:]
        moved = dot3(kept_pieces, tuple(p[:tokens] for p in bk), TN)
        kh, kl = (p[tokens:] for p in bk)
        stored = dot(v, kh, TN) + dot(v, kl, TN)
        eye = (row == col)[:WIDTH, :WIDTH].astype(f32)
        last = decay[tokens - 1 :, cut]
        m_ref[head] = jnp.concatenate(
            [(moved[:WIDTH] + eye) * last, (moved[WIDTH:] + stored) * last], axis=1
        ).astype(bf16)


def chunk(r, k, v, x, l):
    tokens, channels = r.shape
    pair = 2 * WIDTH
    heads = channels // WIDTH
    block = pl.BlockSpec((tokens, pair), lambda i: (0, i))
    return pl.pallas_call(
        chunk_kernel,
        grid=(channels // pair,),
        out_shape=(
            jax.ShapeDtypeStruct((tokens, channels), f32),
            jax.ShapeDtypeStruct((tokens, channels), f32),
            jax.ShapeDtypeStruct((heads, WIDTH, pair), bf16),
        ),
        in_specs=[block] * 5,
        out_specs=(block, block, pl.BlockSpec((2, WIDTH, pair), lambda i: (i, 0, 0))),
        cost_estimate=pl.CostEstimate(
            flops=heads * 200_000_000, bytes_accessed=tokens * channels * 22, transcendentals=0
        ),
        name="chunk",
    )(r, k, v, x, l)


def finish_kernel(me_ref, maps_ref, q_ref, o_ref, r_ref, k_ref, v_ref, g_ref, e_ref, s_ref, w_ref, out_ref, mixed):
    heads = maps_ref.shape[1]

    def step(i, states):
        following = []
        for head in range(heads):
            joined = maps_ref[i, head]
            move, add = joined[:, :WIDTH], joined[:, WIDTH:]
            high, low = split(states[head])
            following.append(dot(high, move) + dot(low, move) + add.astype(f32))
        return tuple(following)

    start = tuple(jnp.zeros((WIDTH, WIDTH), f32) for _ in range(heads))
    states = lax.fori_loop(0, me_ref[0], step, start)
    for head in range(heads):
        cut = slice(head * WIDTH, (head + 1) * WIDTH)
        o = o_ref[:, cut] + dot3(split(q_ref[:, cut]), split(states[head]), NT)
        centred = o - jnp.mean(o, axis=-1, keepdims=True)
        scaled = centred * lax.rsqrt(jnp.mean(centred * centred, axis=-1, keepdims=True) + group_eps)
        r, k, v, g = (a[:, cut].astype(f32) for a in (r_ref, k_ref, v_ref, g_ref))
        bonus = jnp.sum(r * k * e_ref[:, cut], axis=-1, keepdims=True) * v
        mixed[:, cut] = ((scaled * s_ref[:, cut] + bonus) * g).astype(bf16)
    out_ref[...] = dot(mixed[...], w_ref[...]).astype(bf16)


def finish(me, maps, q, o, r, k, v, g, extra, scale, weights):
    tokens, channels = r.shape
    vmem = pl.BlockSpec(memory_space=pltpu.VMEM)
    return pl.pallas_call(
        finish_kernel,
        out_shape=jax.ShapeDtypeStruct((tokens, weights.shape[1]), bf16),
        in_specs=[pl.BlockSpec(memory_space=pltpu.SMEM)] + [vmem] * 10,
        out_specs=vmem,
        scratch_shapes=[pltpu.VMEM((tokens, channels), bf16)],
        cost_estimate=pl.CostEstimate(
            flops=2_000_000_000, bytes_accessed=4_000_000, transcendentals=0
        ),
        name="finish",
    )(me, maps, q, o, r, k, v, g, extra[None], scale[None], weights)


def body(
    r, k, v, x, l, g, extra, scale, exit_weights, skip, gain, gate_w, up_w, taps_w, down_w
):
    token_count = r.shape[0]
    place = lax.axis_index(("z", "p"))

    gate_up = jnp.concatenate([gate_w, up_w], axis=0).reshape((2,) + gate_w.shape)
    gate_up = lax.all_to_all(gate_up, "p", split_axis=2, concat_axis=1, tiled=True)
    down_part = lax.all_to_all(down_w, "p", split_axis=0, concat_axis=1, tiled=True)

    q, o, maps = chunk(r, k, v, x, l)
    maps = lax.all_gather(maps, ("z", "p"))
    gate_full = lax.all_gather(gate_up[0], "z", axis=0, tiled=True)
    up_full = lax.all_gather(gate_up[1], "z", axis=0, tiled=True)
    down_full = lax.all_gather(down_part, "z", axis=1, tiled=True)
    partial = finish(place[None].astype(jnp.int32), maps, q, o, r, k, v, g, extra, scale, exit_weights)
    attended = lax.psum_scatter(partial, "t", scatter_dimension=0, tiled=True).astype(f32)
    hidden_res = skip.astype(f32) + attended
    normed = (
        hidden_res
        * lax.rsqrt(jnp.mean(hidden_res * hidden_res, axis=-1, keepdims=True) + norm_eps)
        * gain
    ).astype(bf16)
    rows = lax.all_gather(normed, ("p", "t"), axis=0, tiled=True)
    gate_pre = jnp.dot(rows, gate_full, preferred_element_type=f32).astype(bf16)
    count, taps = rows.shape[0], taps_w.shape[0]
    groups = lax.axis_size("z")
    tail = lax.ppermute(gate_pre[count - taps + 1 :], "z", [(i, i + 1) for i in range(groups - 1)])
    up_part = jnp.dot(rows, up_full, preferred_element_type=f32).astype(bf16)
    units = gate_pre.shape[1]
    own_taps = lax.dynamic_slice_in_dim(taps_w, lax.axis_index("p") * units, units, 1)
    extended = jnp.concatenate([tail, gate_pre], axis=0).astype(f32)
    conv_out = jnp.zeros(gate_pre.shape, f32)
    for tap in range(taps):
        conv_out = conv_out + own_taps[tap] * extended[tap : tap + count]
    hidden = (jax.nn.silu(conv_out) * up_part.astype(f32)).astype(bf16)
    projected = lax.psum_scatter(
        jnp.dot(hidden, down_full, preferred_element_type=f32).astype(bf16),
        ("p", "t"),
        scatter_dimension=0,
        tiled=True,
    ).astype(f32)
    return (hidden_res + projected).astype(bf16)


def solution(mesh):
    names = mesh.axis_names
    spread, wide = mesh.shape[names[0]], mesh.shape[names[1]]
    group = GROUP if spread % GROUP == 0 else 1
    fine = Mesh(mesh.devices.reshape(spread // group, group, wide), ("z", "p", "t"))
    sp = ("z", "p")
    both = P(sp, "t")
    return jax.shard_map(
        body,
        mesh=fine,
        in_specs=(
            both, both, both, both, both, both,
            P("t"), P("t"), P("t", None),
            P(("z", "p", "t"), None), P(),
            both, both, P(None, "t"), P("t", sp),
        ),
        out_specs=P(("z", "p", "t"), None),
        check_vma=False,
    )
```

time: 1210 us -> 374 us (0.31); the launches traced: 1190 us -> 373 us
  matrix products: 311 us -> 12.5 us
  waiting for transfers between devices: 549 us -> 280 us
  local copies, waits for them, and re-layouts: 248 us -> 8.31 us
  other arithmetic: 64.1 us -> 5.19 us
  Pallas kernels: 0 us -> 28.6 us
  blocking collectives: 2.18 us -> 15 us
    dot_general x79 -> x2, matrix products: 311 us -> 12.5 us  [the longest x1 8.37 us: body(): jnp.dot(hidden, down_full, preferred_element_type=f32).astype(bf16)]
    all_gather x5, waiting for transfers between devices: 500 us -> 226 us  [the longest x1 60.1 us: body(): up_full = lax.all_gather(gate_up[1], 'z', axis=0, tiled=True)]
    pad x8 -> x0, local copies, waits for them, and re-layouts: 86 us -> none  [recurrence(): lax.associative_scan(compose, (block_maps, block_states))]
    dynamic_update_slice x32 -> x0, local copies, waits for them, and re-layouts: 57 us -> none  [recurrence(): lax.scan(span_step, (zero_state, start_maps), arranged)]
    add x22 -> x0, other arithmetic: 45.1 us -> none  [the longest x16 34.4 us: span_step(): mapping * fading[:, :, None, :]]
    pallas_call x0 -> x2, Pallas kernels: none -> 28.6 us  [the longest x1 22.7 us: chunk(): pl.pallas_call(chunk_kernel, grid=(channels // pair,), out_shape=(jax.Sha...]
    mul x36 -> x0, local copies, waits for them, and re-layouts: 25.3 us -> none  [the longest x16 12.7 us: span_step(): along[..., None] * erase_amt[:, :, None, :]]
    while x128 -> x0, local copies, waits for them, and re-layouts: 22.2 us -> none
  transfers between devices with their start and end apart: 8 -> 9, of which waited for: 7 -> 8; matrix products, arithmetic and copies ran while one was open for 7% -> 4% of each run, Pallas kernels for 0% -> 2%
where the time goes in v1:
time: 374 us; the launch traced here: 373 us
  waiting for transfers between devices  280 us (75%)
  Pallas kernels  28.6 us (8%)
  between operations  15.2 us (4%)
  blocking collectives  15 us (4%)
  matrix products  12.5 us (3%)
  starting transfers between devices  9 us (2%)
  local copies, waits for them, and re-layouts  8.31 us (2%)
  other arithmetic  5.19 us (1%)
    all_gather x1, waiting for transfers between devices, body(): up_full = lax.all_gather(gate_up[1], 'z', axis=0, tiled=True)  60.1 us
    all_gather x1, waiting for transfers between devices, body(): maps = lax.all_gather(maps, ('z', 'p'))  59.9 us
    all_gather x1, waiting for transfers between devices, body(): down_full = lax.all_gather(down_part, 'z', axis=1, tiled=True)  45.5 us
    reduce_scatter x1, waiting for transfers between devices, body(): lax.psum_scatter(jnp.dot(hidden, down_full, preferred_element_type=f32).a...  39.8 us
    all_gather x1, waiting for transfers between devices, body(): gate_full = lax.all_gather(gate_up[0], 'z', axis=0, tiled=True)  32.3 us
    all_gather x1, waiting for transfers between devices, body(): rows = lax.all_gather(normed, ('p', 't'), axis=0, tiled=True)  28.1 us
    pallas_call x1, Pallas kernels, chunk(): pl.pallas_call(chunk_kernel, grid=(channels // pair,), out_shape=(jax.Sha...  22.7 us
    all_to_all x1, blocking collectives, body(): lax.all_to_all(down_w, 'p', split_axis=0, concat_axis=1, tiled=True)  15 us
  transfers between devices with their start and end apart: 9, of which 8 were waited for; matrix products, arithmetic and copies ran while one was open for 4% of the time, Pallas kernels for 2%

profile of v1, /device:TPU:0, one launch (start us, length us, event | category | flops | bytes accessed | tf_op | source)
XLA Modules:
  0.0 373.5 jit_solution(4545904982395002972)
XLA Ops:
  7.4 22.7 %chunk.1 = (f32[128,512]{1,0:T(8,128)}, f32[128,512]{1,0:T(8,128)}, bf16[8,64,128]{2,1,0:T(8,128)(2,1)}) custom-call(bf16[128,512]{1,0:T(8,128)(2,1)} %r_ref.3, bf16[128,512]{1,0:T(8,128)(2,1)} %k_ref.3, bf16[128,512]{1,0:T(8,128)(2,1)} %v_ref.3, f32[128,512]{1,0:T(8,128)} %x_ref.1, f32[128,512]{1,0:T(8,128)} %l_ref.1), custom_call_target="tpu_custom_call" | custom-call | flops 1600000000 | bytes 1441792 | tf_op jit(solution)/shard_map/chunk/pallas_call | solution.py:100
  30.1 0.0 all-gather.15.cloned.1.call-update
  30.1 0.0 copy-done.3
  30.1 0.0 copy-done.4
  30.2 0.1 pad_maximum_fusion
  30.3 2.9 copy.23
  33.2 5.2 %all-to-all-start = ((bf16[2,128,2816]{1,0,2:T(2,128)(2,1)}), bf16[2,128,2816]{1,0,2:T(2,128)(2,1)S(1)}, u32[]{:S(2)}, u32[]{:S(2)}) async-start(bf16[2,128,2816]{1,0,2:T(2,128)(2,1)} %copy.23), calls=%async_computation.1 | async-start | bytes 2883584 | tf_op jit(solution)/shard_map/all_to_all | solution.py:165
  38.4 59.9 %all-gather.15.cloned.1.call-done = bf16[128,64,128]{2,1,0:T(8,128)(2,1)} async-done(((bf16[8,64,128]{2,1,0:T(8,128)(2,1)}), bf16[128,64,128]{2,1,0:T(8,128)(2,1)}) %all-gather.15.cloned.1.call-update) | async-done | bytes 2097168 | tf_op jit(solution)/shard_map/all_gather | solution.py:169
  98.3 5.8 %finish.1 = bf16[128,2048]{1,0:T(8,128)(2,1)} custom-call(s32[1]{0:T(128)} %bitcast.me_ref, bf16[16,8,64,128]{3,2,1,0:T(8,128)(2,1)} %bitcast.41, f32[128,512]{1,0:T(8,128)} %get-tuple-element.9.q_ref, f32[128,512]{1,0:T(8,128)} %get-tuple-element.10.o_ref, bf16[128,512]{1,0:T(8,128)(2,1)} %r_ref.3, bf16[128,512]{1,0:T(8,128)(2,1)} %k_ref.3, ...), custom_call_target="tpu_custom_call" | custom-call | flops 2000000000 | bytes 4000000 | tf_op jit(solution)/shard_map/finish/pallas_call | solution.py:145
  104.1 0.0 reduce-scatter.3.cloned.1.call-update
  104.1 0.0 all-gather.9.cloned.1.call-start
  104.2 0.0 all-to-all-done
  104.2 0.2 copy.24
  104.4 0.1 fusion.7
  104.5 0.0 copy-start
  104.5 0.0 copy-start.5
  104.5 0.6 copy.25
  105.1 0.0 copy-start.2
  105.1 1.0 copy.35
  106.1 0.0 all-gather.9.cloned.1.call-update
  106.1 0.0 all-gather.7.cloned.1.call-start
  106.2 8.2 %reduce-scatter.3.cloned.1.call-done = bf16[64,2048]{1,0:T(8,128)(2,1)} async-done(((bf16[128,2048]{1,0:T(8,128)(2,1)}), bf16[64,2048]{1,0:T(8,128)(2,1)}) %reduce-scatter.3.cloned.1.call-update) | async-done | bytes 262160 | tf_op jit(solution)/shard_map/reduce_scatter | solution.py:174
  114.4 1.2 multiply_reduce_fusion
  115.5 1.8 multiply_convert_fusion.1
  117.3 0.0 all-gather.7.cloned.1.call-update
  117.4 0.0 all-gather.13.cloned.1.call-start
  117.4 15.0 %all_to_all.34 = bf16[4,704,128]{2,1,0:T(8,128)(2,1)S(1)} all-to-all(bf16[4,704,128]{2,1,0:T(8,128)(2,1)S(1)} %bitcast.40), channel_id=1, replica_groups=mesh['z'=4,'p'=4,'t'=2] {'p'}, dimensions={0} | all-to-all | bytes 1441792 | tf_op jit(solution)/shard_map/all_to_all | solution.py:166
  132.4 0.9 copy_bitcast_fusion.2
  133.3 0.0 all-gather.13.cloned.1.call-update
  133.3 0.0 all-gather.11.cloned.1.call-start
  133.4 0.6 copy.26
  134.0 1.0 copy.34
  135.0 0.0 all-gather.11.cloned.1.call-update
  135.0 0.0 reduce-scatter.5.cloned.1.call-start
  135.0 32.3 %all-gather.9.cloned.1.call-done = bf16[2048,704]{0,1:T(8,128)(2,1)} async-done(((bf16[512,704]{0,1:T(8,128)(2,1)}), bf16[2048,704]{0,1:T(8,128)(2,1)}) %all-gather.9.cloned.1.call-update) | async-done | bytes 2883600 | tf_op jit(solution)/shard_map/all_gather | solution.py:170
  167.3 28.1 %all-gather.7.cloned.1.call-done = bf16[512,2048]{1,0:T(8,128)(2,1)} async-done(((bf16[64,2048]{1,0:T(8,128)(2,1)}), bf16[512,2048]{1,0:T(8,128)(2,1)}) %all-gather.7.cloned.1.call-update) | async-done | bytes 2097168 | tf_op jit(solution)/shard_map/all_gather | solution.py:181
  195.5 4.1 %convolution_convert_fusion.2 = bf16[512,704]{0,1:T(8,128)(2,1)S(1)} fusion(bf16[512,2048]{1,0:T(8,128)(2,1)} %all-gather.7.cloned.1.call-done, bf16[2048,704]{0,1:T(8,128)(2,1)} %all-gather.9.cloned.1.call-done), kind=kOutput, calls=%fused_computation.9 | convolution fusion | flops 1476755456 | bytes 5701632 | tf_op jit(solution)/shard_map/dot_general | solution.py:182
  199.6 0.1 slice.39
  199.7 3.6 collective-permute-start
  203.3 0.9 dynamic-slice_reduce_fusion.2
  204.2 5.8 %collective-permute-done = bf16[2,704]{0,1:T(8,128)(2,1)S(1)} collective-permute-done((bf16[2,704]{0,1:T(8,128)(2,1)S(1)}, bf16[2,704]{0,1:T(8,128)(2,1)S(1)}, u32[]{:S(2)}, u32[]{:S(2)}) %collective-permute-start) | collective-permute-done | bytes 2848 | tf_op jit(solution)/shard_map/ppermute | solution.py:185
  210.1 0.4 maximum_convert_fusion
  210.5 45.5 %all-gather.13.cloned.1.call-done = bf16[704,2048]{1,0:T(8,128)(2,1)} async-done(((bf16[704,512]{1,0:T(8,128)(2,1)}), bf16[704,2048]{1,0:T(8,128)(2,1)}) %all-gather.13.cloned.1.call-update) | async-done | bytes 2883600 | tf_op jit(solution)/shard_map/all_gather | solution.py:172
  255.9 60.1 %all-gather.11.cloned.1.call-done = bf16[2048,704]{0,1:T(8,128)(2,1)} async-done(((bf16[512,704]{0,1:T(8,128)(2,1)}), bf16[2048,704]{0,1:T(8,128)(2,1)}) %all-gather.11.cloned.1.call-update) | async-done | bytes 2883600 | tf_op jit(solution)/shard_map/all_gather | solution.py:171
  316.0 8.4 %convolution_convert_fusion = bf16[512,2048]{1,0:T(8,128)(2,1)} fusion(bf16[704,2048]{1,0:T(8,128)(2,1)} %all-gather.13.cloned.1.call-done, f32[514,704]{0,1:T(8,128)S(1)} %maximum_convert_fusion, bf16[512,2048]{1,0:T(8,128)(2,1)} %all-gather.7.cloned.1.call-done, bf16[2048,704]{0,1:T(8,128)(2,1)} %all-gather.11.cloned.1.call-done, ...), kind=kOutput, calls=%fused_computation | convolution fusion | flops 2958524416 | bytes 14299136 | tf_op jit(solution)/shard_map/dot_general | solution.py:195
  324.3 0.0 reduce-scatter.5.cloned.1.call-update
  324.4 39.8 %reduce-scatter.5.cloned.1.call-done = bf16[64,2048]{1,0:T(8,128)(2,1)} async-done(((bf16[512,2048]{1,0:T(8,128)(2,1)}), bf16[64,2048]{1,0:T(8,128)(2,1)}) %reduce-scatter.5.cloned.1.call-update) | async-done | bytes 262160 | tf_op jit(solution)/shard_map/reduce_scatter | solution.py:194
  364.1 1.7 add_convert_fusion
  (10 shorter events, 0.0 us)
Async XLA Ops:
  7.4 22.8 %copy-start.3 = (bf16[128,2816]{1,0:T(8,128)(2,1)S(1)}, bf16[128,2816]{1,0:T(8,128)(2,1)}, u32[]{:S(2)}) copy-start(bf16[128,2816]{1,0:T(8,128)(2,1)} %param.27) | copy-start | bytes 2162692
  7.4 22.8 %copy-start.4 = (bf16[128,2816]{1,0:T(8,128)(2,1)S(1)}, bf16[128,2816]{1,0:T(8,128)(2,1)}, u32[]{:S(2)}) copy-start(bf16[128,2816]{1,0:T(8,128)(2,1)} %param.26) | copy-start | bytes 2162692
  7.4 90.9 %all-gather.15.cloned.1.call-start = ((), (), s32[]{:S(2)}) async-start(), calls=%async_computation.10 | async-start | bytes 2228224 | tf_op jit(solution)/shard_map/all_gather | solution.py:169
  33.2 71.0 %all-to-all-start = ((bf16[2,128,2816]{1,0,2:T(2,128)(2,1)}), bf16[2,128,2816]{1,0,2:T(2,128)(2,1)S(1)}, u32[]{:S(2)}, u32[]{:S(2)}) async-start(bf16[2,128,2816]{1,0,2:T(2,128)(2,1)} %copy.23), calls=%async_computation.1 | async-start | bytes 2883584 | tf_op jit(solution)/shard_map/all_to_all | solution.py:165
  38.4 76.0 %reduce-scatter.3.cloned.1.call-start = ((), (), s32[]{:S(2)}) async-start(), calls=%async_computation.4 | async-start | bytes 786432 | tf_op jit(solution)/shard_map/reduce_scatter | solution.py:174
  104.1 63.2 %all-gather.9.cloned.1.call-start = ((), (), s32[]{:S(2)}) async-start(), calls=%async_computation.6 | async-start | bytes 3604480 | tf_op jit(solution)/shard_map/all_gather | solution.py:170
  104.5 9.9 %copy-start = (bf16[64,2048]{1,0:T(8,128)(2,1)S(1)}, bf16[64,2048]{1,0:T(8,128)(2,1)}, u32[]{:S(2)}) copy-start(bf16[64,2048]{1,0:T(8,128)(2,1)} %param.24) | copy-start | bytes 786436
  104.5 11.0 %copy-start.5 = (f32[2048]{0:T(1024)S(1)}, f32[2048]{0:T(1024)}, u32[]{:S(2)}) copy-start(f32[2048]{0:T(1024)} %param.25) | copy-start | bytes 24580
  105.1 12.3 %copy-start.2 = (bf16[2816,128]{1,0:T(8,128)(2,1)S(1)}, bf16[2816,128]{1,0:T(8,128)(2,1)}, u32[]{:S(2)}) copy-start(bf16[2816,128]{1,0:T(8,128)(2,1)} %param.29) | copy-start | bytes 2162692
  106.1 89.4 %all-gather.7.cloned.1.call-start = ((), (), s32[]{:S(2)}) async-start(), calls=%async_computation.5 | async-start | bytes 2359296 | tf_op jit(solution)/shard_map/all_gather | solution.py:181
  117.4 138.5 %all-gather.13.cloned.1.call-start = ((), (), s32[]{:S(2)}) async-start(), calls=%async_computation.8 | async-start | bytes 3604480 | tf_op jit(solution)/shard_map/all_gather | solution.py:172
  133.3 182.6 %all-gather.11.cloned.1.call-start = ((), (), s32[]{:S(2)}) async-start(), calls=%async_computation.7 | async-start | bytes 3604480 | tf_op jit(solution)/shard_map/all_gather | solution.py:171
  135.0 229.1 %reduce-scatter.5.cloned.1.call-start = ((), (), s32[]{:S(2)}) async-start(), calls=%async_computation.9 | async-start | bytes 2359296 | tf_op jit(solution)/shard_map/reduce_scatter | solution.py:194
  199.7 10.3 %collective-permute-start = (bf16[2,704]{0,1:T(8,128)(2,1)S(1)}, bf16[2,704]{0,1:T(8,128)(2,1)S(1)}, u32[]{:S(2)}, u32[]{:S(2)}) collective-permute-start(bf16[2,704]{0,1:T(8,128)(2,1)S(1)} %slice.39), channel_id=1, source_target_pairs={{0,8},{8,16},{16,24},{1,9},{9,17},{17,25},{2,10},{10,18},{18,26},{... | collective-permute-start | bytes 8456 | tf_op jit(solution)/shard_map/ppermute | solution.py:185
  324.3 39.8 %copy-start.1 = (bf16[64,2048]{1,0:T(8,128)(2,1)S(1)}, bf16[64,2048]{1,0:T(8,128)(2,1)}, u32[]{:S(2)}) copy-start(bf16[64,2048]{1,0:T(8,128)(2,1)} %reduce-scatter.3.cloned.1.call-done) | copy-start | bytes 786436
Sparse Core Ops, SparseCore 0:
  30.3 67.9 all-gather.14
  104.2 10.0 reduce-scatter.2
Sparse Core Ops, SparseCore 1:
  106.2 61.1 all-gather.8
  169.1 26.3 all-gather.6
  196.9 58.9 all-gather.12
  257.5 58.4 all-gather.10
  324.4 39.6 reduce-scatter.4

commit v2 on v1

v2 whole, which is shorter than its diff:
```python
import functools

import jax
import jax.numpy as jnp
from jax import lax
from jax.experimental import pallas as pl
from jax.experimental.pallas import tpu as pltpu
from jax.sharding import Mesh, PartitionSpec as P

WIDTH = 64
GROUP = 4
group_eps = 0.00064
norm_eps = 1e-06
f32, bf16 = jnp.float32, jnp.bfloat16
NN, NT, TN = ((1,), (0,)), ((1,), (1,)), ((0,), (0,))


def split(a):
    high = a.astype(bf16)
    return high, (a - high.astype(f32)).astype(bf16)


def dot(a, b, dims=NN):
    return lax.dot_general(a, b, (dims, ((), ())), preferred_element_type=f32)


def dot3(a, b, dims=NN):
    (ah, al), (bh, bl) = a, b
    return dot(ah, bh, dims) + (dot(ah, bl, dims) + dot(al, bh, dims))


MESH = pl.DeviceIdType.MESH


def others(axis):
    size, me = lax.axis_size(axis), lax.axis_index(axis)
    return [(lax.rem(me + d, size), lax.rem(me + size - d, size)) for d in range(1, size)]


def peers(kinds):
    found = []
    for kind in kinds:
        if kind[0] == "oa":
            found += outer_peers()[0]
        else:
            found += [{kind[0]: to} for to, _ in others(kind[0])]
    return found


def outer_peers():
    count, size = lax.axis_size("o") * lax.axis_size("a"), lax.axis_size("a")
    me = lax.axis_index("o") * size + lax.axis_index("a")
    to, come = [], []
    for d in range(1, count):
        there = lax.rem(me + d, count)
        to.append({"o": there // size, "a": lax.rem(there, size)})
        come.append(lax.rem(me + count - d, count))
    return to, come, me


def greet(kinds):
    barrier = pltpu.get_barrier_semaphore()
    who = peers(kinds)
    for device in who:
        pl.semaphore_signal(barrier, inc=1, device_id=device, device_id_type=MESH)
    pl.semaphore_wait(barrier, len(who))


def remote(src, dst, send, recv, device):
    return pltpu.make_async_remote_copy(
        src_ref=src, dst_ref=dst, send_sem=send, recv_sem=recv, device_id=device, device_id_type=MESH
    )


def exchange(sources, targets, sends, recvs, local, begin):
    me = lax.axis_index("a")
    for n, (src, dst) in enumerate(zip(sources, targets)):
        own = pltpu.make_async_copy(src.at[me], dst.at[me], local.at[n])
        if begin:
            own.start()
        for d, (to, come) in enumerate(others("a")):
            out = remote(src.at[to], dst.at[me], sends.at[n, d], recvs.at[n, me], {"a": to})
            if begin:
                out.start()
            else:
                out.wait_send()
                remote(src.at[to], dst.at[come], sends.at[n, d], recvs.at[n, come], {"a": to}).wait_recv()
        if not begin:
            own.wait()


def chunk_kernel(r_ref, k_ref, v_ref, x_ref, l_ref, gate, up, down, q_ref, o_ref, m_ref, gate_out, up_out, down_out, sends, recvs, local):
    swap = functools.partial(exchange, (gate, up, down), (gate_out, up_out, down_out), sends, recvs, local)

    @pl.when(pl.program_id(0) == 0)
    def _():
        greet([("a",)])
        swap(True)

    tokens, lanes = r_ref.shape
    row = lax.broadcasted_iota(jnp.int32, (tokens, tokens), 0)
    col = lax.broadcasted_iota(jnp.int32, (tokens, tokens), 1)
    log_decay = -jax.nn.sigmoid(x_ref[...]) * jnp.exp(jnp.asarray(-0.5, f32))
    ones = (row >= col).astype(bf16)
    d0, rest = split(log_decay)[0], log_decay
    rest = log_decay - d0.astype(f32)
    d1, d2 = split(rest)
    running = dot(ones, d0) + (dot(ones, d1) + dot(ones, d2))
    decay = jnp.exp(running)
    before = jnp.exp(running - log_decay)
    inverse = jnp.exp(-running)
    rate = jax.nn.sigmoid(l_ref[...])
    r_all, k_all, v_all = (a[...].astype(f32) for a in (r_ref, k_ref, v_ref))
    k_hat_all = k_all * inverse
    r_hat_all = r_all * decay
    for head in range(lanes // WIDTH):
        cut = slice(head * WIDTH, (head + 1) * WIDTH)
        k = k_all[:, cut]
        length = jnp.sqrt(jnp.sum(k * k, axis=-1, keepdims=True))
        unit = k / jnp.maximum(length, 1.0)
        a_hat = -unit * before[:, cut]
        b_hat = unit * rate[:, cut] * inverse[:, cut]
        k_hat, r_hat = k_hat_all[:, cut], r_hat_all[:, cut]
        v = v_ref[:, cut]
        bk = split(jnp.concatenate([b_hat, k_hat], axis=0))
        both = dot3(split(jnp.concatenate([a_hat, r_hat], axis=0)), bk, NT)
        erase = jnp.where(row > col, both[:tokens, :tokens], 0.0)
        write = jnp.where(row > col, both[:tokens, tokens:], 0.0)
        out_erase = jnp.where(row >= col, both[tokens:, :tokens], 0.0)
        out_write = jnp.where(row >= col, both[tokens:, tokens:], 0.0)
        solved = (row == col).astype(f32)
        block = 1
        while block < tokens:
            off = (row // block == col // block + 1) & (row // (2 * block) == col // (2 * block))
            part = jnp.where(off, erase, 0.0)
            if block == 1:
                solved = solved + part
            else:
                pieces = split(solved)
                solved = solved + dot3(split(dot3(pieces, split(part))), pieces)
            block *= 2
        wh, wl = split(write)
        seen = jnp.concatenate([a_hat, dot(wh, v) + dot(wl, v)], axis=1)
        kept = dot3(split(solved), split(seen))
        kept_pieces = split(kept)
        oh, ol = split(out_write)
        out = dot3(split(out_erase), kept_pieces) + jnp.concatenate(
            [r_hat, dot(oh, v) + dot(ol, v)], axis=1
        )
        q_ref[:, cut] = out[:, :WIDTH]
        o_ref[:, cut] = out[:, WIDTH:]
        moved = dot3(kept_pieces, tuple(p[:tokens] for p in bk), TN)
        kh, kl = (p[tokens:] for p in bk)
        stored = dot(v, kh, TN) + dot(v, kl, TN)
        eye = (row == col)[:WIDTH, :WIDTH].astype(f32)
        last = decay[tokens - 1 :, cut]
        m_ref[head] = jnp.concatenate(
            [(moved[:WIDTH] + eye) * last, (moved[WIDTH:] + stored) * last], axis=1
        ).astype(bf16)

    @pl.when(pl.program_id(0) == pl.num_programs(0) - 1)
    def _():
        swap(False)


def chunk(r, k, v, x, l, gate, up, down):
    tokens, channels = r.shape
    pair = 2 * WIDTH
    heads = channels // WIDTH
    size = gate.shape[0]
    block = pl.BlockSpec((tokens, pair), lambda i: (0, i))
    hbm = pl.BlockSpec(memory_space=pltpu.HBM)
    return pl.pallas_call(
        chunk_kernel,
        grid=(channels // pair,),
        out_shape=(
            jax.ShapeDtypeStruct((tokens, channels), f32),
            jax.ShapeDtypeStruct((tokens, channels), f32),
            jax.ShapeDtypeStruct((heads, WIDTH, pair), bf16),
        )
        + tuple(jax.ShapeDtypeStruct(w.shape, bf16) for w in (gate, up, down)),
        in_specs=[block] * 5 + [hbm] * 3,
        out_specs=(block, block, pl.BlockSpec((2, WIDTH, pair), lambda i: (i, 0, 0)), hbm, hbm, hbm),
        scratch_shapes=[
            pltpu.SemaphoreType.DMA((3, size)),
            pltpu.SemaphoreType.DMA((3, size)),
            pltpu.SemaphoreType.DMA((3,)),
        ],
        compiler_params=pltpu.CompilerParams(collective_id=0, has_side_effects=True),
        cost_estimate=pl.CostEstimate(
            flops=heads * 200_000_000, bytes_accessed=tokens * channels * 22, transcendentals=0
        ),
        name="chunk",
    )(r, k, v, x, l, gate, up, down)


def finish_kernel(
    m_ref, q_ref, o_ref, r_ref, k_ref, v_ref, g_ref, e_ref, s_ref, w_ref, skip_ref, gain_ref,
    rows_ref, res_ref,
    near, total, far, mixed, partial, parts, near_s, near_r, far_s, far_r, part_s, part_r, row_s, row_r, pass_s,
):
    heads = m_ref.shape[0]
    side, across = lax.axis_size("b"), far.shape[0]
    b, a, t = lax.axis_index("b"), lax.axis_index("a"), lax.axis_index("t")
    wide = lax.axis_size("t")
    greet([("b",), ("oa",), ("t",)])

    sent = []
    for d, (to, come) in enumerate(others("b")):
        copy = remote(m_ref, near.at[b], near_s.at[d], near_r.at[b], {"b": to})
        copy.start()
        sent.append(copy)
    for to, come in others("b"):
        remote(m_ref, near.at[come], near_s.at[0], near_r.at[come], {"b": to}).wait_recv()
    near[b] = m_ref[...]
    eye = (
        lax.broadcasted_iota(jnp.int32, (2 * WIDTH, WIDTH), 0)
        == lax.broadcasted_iota(jnp.int32, (2 * WIDTH, WIDTH), 1)
    ).astype(f32)
    befores = [eye] * heads
    for head in range(heads):
        running = None
        for i in range(side):
            joined = near[i, head]
            move, add = joined[:, :WIDTH], joined[:, WIDTH:]
            if running is None:
                running = jnp.concatenate([move, add], axis=0).astype(f32)
            else:
                befores[head] = jnp.where(b == i, running, befores[head])
                high, low = split(running)
                running = dot(high, move) + dot(low, move)
                running = running + jnp.concatenate(
                    [jnp.zeros((WIDTH, WIDTH), f32), add.astype(f32)], axis=0
                )
        total[head] = jnp.concatenate([running[:WIDTH], running[WIDTH:]], axis=1).astype(bf16)

    to_outer, come_outer, outer = outer_peers()
    for d, device in enumerate(to_outer):
        copy = remote(total, far.at[outer], far_s.at[d], far_r.at[outer], device)
        copy.start()
        sent.append(copy)
    for come, device in zip(come_outer, to_outer):
        remote(total, far.at[come], far_s.at[0], far_r.at[come], device).wait_recv()
    far[outer] = total[...]
    for head in range(heads):
        state = jnp.zeros((WIDTH, WIDTH), f32)
        for i in range(across - 1):
            joined = far[i, head]
            high, low = split(state)
            following = dot(high, joined[:, :WIDTH]) + dot(low, joined[:, :WIDTH])
            state = jnp.where(i < outer, following + joined[:, WIDTH:].astype(f32), state)
        state = dot3(split(state), split(befores[head][:WIDTH])) + befores[head][WIDTH:]
        cut = slice(head * WIDTH, (head + 1) * WIDTH)
        o = o_ref[:, cut] + dot3(split(q_ref[:, cut]), split(state), NT)
        centred = o - jnp.mean(o, axis=-1, keepdims=True)
        scaled = centred * lax.rsqrt(jnp.mean(centred * centred, axis=-1, keepdims=True) + group_eps)
        r, k, v, g = (x[:, cut].astype(f32) for x in (r_ref, k_ref, v_ref, g_ref))
        bonus = jnp.sum(r * k * e_ref[:, cut], axis=-1, keepdims=True) * v
        mixed[:, cut] = ((scaled * s_ref[:, cut] + bonus) * g).astype(bf16)

    own = skip_ref.shape[0]
    product = dot(mixed[...], w_ref[...]).astype(bf16)
    for n in range(wide):
        partial[n] = product[n * own : (n + 1) * own]
    for d, (to, come) in enumerate(others("t")):
        copy = remote(partial.at[to], parts.at[t], part_s.at[d], part_r.at[t], {"t": to})
        copy.start()
        sent.append(copy)
    for to, come in others("t"):
        remote(partial.at[to], parts.at[come], part_s.at[0], part_r.at[come], {"t": to}).wait_recv()
    parts[t] = partial[t]
    hidden_res = skip_ref[...].astype(f32)
    attended = parts[0].astype(f32)
    for n in range(1, wide):
        attended = attended + parts[n].astype(f32)
    hidden_res = hidden_res + attended
    res_ref[...] = hidden_res
    normed = (
        hidden_res
        * lax.rsqrt(jnp.mean(hidden_res * hidden_res, axis=-1, keepdims=True) + norm_eps)
        * gain_ref[...]
    )
    normed = normed.astype(bf16)
    outers, along = lax.axis_size("o"), lax.axis_size("a")
    piece = normed.shape[1] // (outers * along * side)
    starts = [((i * along + j) * side + n) * piece for i in range(outers) for n in range(side) for j in range(along)]
    rows_ref[a, t] = jnp.concatenate([normed[:, at : at + piece] for at in starts], axis=1)

    def give(slot, send, device):
        copy = remote(rows_ref.at[slot, t], rows_ref.at[slot, t], send, row_r.at[slot, t], device)
        copy.start()
        sent.append(copy)

    for d, (to, come) in enumerate(others("a")):
        give(a, row_s.at[d], {"a": to})
    for d, (to, come) in enumerate(others("t")):
        give(a, pass_s.at[0, d], {"t": to})
    for d, (to, come) in enumerate(others("a")):
        mine = rows_ref.at[come, t]
        remote(mine, mine, row_s.at[0], row_r.at[come, t], {"a": to}).wait_recv()
        for f, (fro, _) in enumerate(others("t")):
            give(come, pass_s.at[d + 1, f], {"t": fro})
    for i in range(lax.axis_size("a")):
        for to, come in others("t"):
            theirs = rows_ref.at[i, come]
            remote(theirs, theirs, row_s.at[0], row_r.at[i, come], {"t": to}).wait_recv()
    for copy in sent:
        copy.wait_send()


def finish(m, q, o, r, k, v, g, extra, scale, weights, skip, gain):
    tokens, channels = r.shape
    own, model = skip.shape
    side, along, wide = (lax.axis_size(x) for x in ("b", "a", "t"))
    across = lax.axis_size("o") * along
    vmem = pl.BlockSpec(memory_space=pltpu.VMEM)
    dma = pltpu.SemaphoreType.DMA
    return pl.pallas_call(
        finish_kernel,
        out_shape=(
            jax.ShapeDtypeStruct((along, wide, own, model), bf16),
            jax.ShapeDtypeStruct((own, model), f32),
        ),
        in_specs=[vmem] * 12,
        out_specs=(vmem, vmem),
        scratch_shapes=[
            pltpu.VMEM((side,) + m.shape, bf16),
            pltpu.VMEM(m.shape, bf16),
            pltpu.VMEM((across,) + m.shape, bf16),
            pltpu.VMEM((tokens, channels), bf16),
            pltpu.VMEM((wide, own, model), bf16),
            pltpu.VMEM((wide, own, model), bf16),
            dma((side,)), dma((side,)), dma((across,)), dma((across,)),
            dma((wide,)), dma((wide,)), dma((along,)), dma((along, wide)), dma((along, wide)),
        ],
        compiler_params=pltpu.CompilerParams(collective_id=1, has_side_effects=True),
        cost_estimate=pl.CostEstimate(
            flops=20_000_000_000, bytes_accessed=4_000_000, transcendentals=0
        ),
        name="finish",
    )(m, q, o, r, k, v, g, extra[None], scale[None], weights, skip, gain[None])


def body(
    r, k, v, x, l, g, extra, scale, exit_weights, skip, gain, gate_w, up_w, taps_w, down_w
):
    tokens = r.shape[0]
    along, side = lax.axis_size("a"), lax.axis_size("b")
    outer = lax.axis_size("o")
    piece = gate_w.shape[0]
    units = gate_w.shape[1] // along

    def by_owner(w):
        return jnp.moveaxis(w.reshape(piece, along, units), 1, 0)

    q, o, m, gate_part, up_part, down_part = chunk(
        r, k, v, x, l, by_owner(gate_w), by_owner(up_w), down_w.reshape(along, units, piece)
    )
    gate_full = lax.all_gather(gate_part, ("o", "b"), axis=0, tiled=True)
    up_full = lax.all_gather(up_part, ("o", "b"), axis=0, tiled=True)
    down_full = lax.all_gather(down_part, ("o", "b"), axis=0, tiled=True)
    rows, hidden_res = finish(
        m, q, o, r, k, v, g, extra, scale, exit_weights, skip, gain
    )
    rows = rows.reshape(along * tokens, -1)
    model = rows.shape[1]
    gate_full, up_full = gate_full.reshape(model, units), up_full.reshape(model, units)
    gate_pre = jnp.dot(rows, gate_full, preferred_element_type=f32).astype(bf16)
    gate_pre = gate_pre.reshape(along, tokens, units)
    reach = taps_w.shape[0] - 1
    tail = gate_pre[:, tokens - reach :]
    tail = lax.ppermute(tail, "b", [(i, (i + 1) % side) for i in range(side)])
    if outer > 1:
        first = lax.ppermute(tail[-1:], "o", [(i, i + 1) for i in range(outer - 1)])
    else:
        first = jnp.zeros_like(tail[:1])
    later = jnp.concatenate([first, tail[:-1]], axis=0)
    tail = jnp.where(lax.axis_index("b") == 0, later, tail)
    up_out = jnp.dot(rows, up_full, preferred_element_type=f32).astype(bf16)
    own_taps = lax.dynamic_slice_in_dim(taps_w, lax.axis_index("a") * units, units, 1)
    extended = jnp.concatenate([tail, gate_pre], axis=1).astype(f32)
    conv_out = jnp.zeros(gate_pre.shape, f32)
    for tap in range(reach + 1):
        conv_out = conv_out + own_taps[tap] * extended[:, tap : tap + tokens]
    hidden = (jax.nn.silu(conv_out).reshape(up_out.shape) * up_out.astype(f32)).astype(bf16)
    down_full = jnp.moveaxis(down_full.reshape(outer, side, along, units, piece), 3, 0)
    down_full = jnp.swapaxes(down_full, 2, 3).reshape(units, model)
    projected = lax.psum_scatter(
        jnp.dot(hidden, down_full, preferred_element_type=f32).astype(bf16),
        ("a", "t"),
        scatter_dimension=0,
        tiled=True,
    ).astype(f32)
    return (hidden_res + projected).astype(bf16)


def solution(mesh):
    names = mesh.axis_names
    spread, wide = mesh.shape[names[0]], mesh.shape[names[1]]
    side = GROUP if spread % GROUP == 0 else 1
    along = GROUP if spread % (side * GROUP) == 0 else 1
    outer = spread // (side * along)
    fine = Mesh(mesh.devices.reshape(outer, along, side, wide), ("o", "a", "b", "t"))
    sp = ("o", "a", "b")
    both = P(sp, "t")
    every = P(sp + ("t",), None)
    return jax.shard_map(
        body,
        mesh=fine,
        in_specs=(
            both, both, both, both, both, both,
            P("t"), P("t"), P("t", None),
            every, P(),
            both, both, P(None, "t"), P("t", sp),
        ),
        out_specs=every,
        check_vma=False,
    )
```

time: 374 us -> 253 us (0.68)
  waiting for transfers between devices: 280 us -> 89.9 us
  Pallas kernels: 28.6 us -> 109 us
  blocking collectives: 15 us -> 0 us
  local copies, waits for them, and re-layouts: 8.31 us -> 17.6 us
  starting transfers between devices: 9 us -> 1.86 us
  other arithmetic: 5.19 us -> 9.38 us
    all_gather x5 -> x3, waiting for transfers between devices: 226 us -> 53 us  [the longest x1 28 us: body(): up_full = lax.all_gather(up_part, ('o', 'b'), axis=0, tiled=True)]
    pallas_call x1, Pallas kernels: 5.83 us -> 55.7 us  [finish(): pl.pallas_call(finish_kernel, out_shape=(jax.ShapeDtypeStruct((along, wid...]
    pallas_call x1, Pallas kernels: 22.7 us -> 53.6 us  [chunk(): pl.pallas_call(chunk_kernel, grid=(channels // pair,), out_shape=(jax.Sha...]
    all_to_all x1 -> x0, blocking collectives: 15 us -> none  [body(): lax.all_to_all(down_w, 'p', split_axis=0, concat_axis=1, tiled=True)]
    reduce_scatter x1 -> x0, waiting for transfers between devices: 8.21 us -> none  [body(): lax.psum_scatter(partial, 't', scatter_dimension=0, tiled=True).astype(f32)]
    reshape x1 -> x5, local copies, waits for them, and re-layouts: 2.92 us -> 9.92 us  [the longest x1 4.04 us: body(): down_full.reshape(outer, side, along, units, piece)]
    ppermute x1, waiting for transfers between devices: 5.81 us -> 0.01 us  [body(): tail = lax.ppermute(tail, 'b', [(i, (i + 1) % side) for i in range(side)])]
    mul x0 -> x1, other arithmetic: none -> 5.27 us  [body(): jax.nn.silu(conv_out).reshape(up_out.shape) * up_out.astype(f32)]
  transfers between devices with their start and end apart: 9 -> 5, of which waited for: 8 -> 3; matrix products, arithmetic and copies ran while one was open for 4% -> 9% of each run, Pallas kernels for 2% -> 22%
where the time goes in v2:
time: 253 us
  Pallas kernels  109 us (43%)
  waiting for transfers between devices  89.9 us (36%)
  local copies, waits for them, and re-layouts  17.6 us (7%)
  between operations  13.2 us (5%)
  matrix products  11.8 us (5%)
  other arithmetic  9.38 us (4%)
    pallas_call x1, Pallas kernels, finish(): pl.pallas_call(finish_kernel, out_shape=(jax.ShapeDtypeStruct((along, wid...  55.7 us
    pallas_call x1, Pallas kernels, chunk(): pl.pallas_call(chunk_kernel, grid=(channels // pair,), out_shape=(jax.Sha...  53.6 us
    reduce_scatter x1, waiting for transfers between devices, body(): lax.psum_scatter(jnp.dot(hidden, down_full, preferred_element_type=f32).a...  36.2 us
    all_gather x1, waiting for transfers between devices, body(): up_full = lax.all_gather(up_part, ('o', 'b'), axis=0, tiled=True)  28 us
    all_gather x1, waiting for transfers between devices, body(): down_full = lax.all_gather(down_part, ('o', 'b'), axis=0, tiled=True)  25 us
    dot_general x1, matrix products, body(): jnp.dot(hidden, down_full, preferred_element_type=f32).astype(bf16)  7.63 us
    mul x1, other arithmetic, body(): jax.nn.silu(conv_out).reshape(up_out.shape) * up_out.astype(f32)  5.27 us
  transfers between devices with their start and end apart: 5, of which 3 were waited for; matrix products, arithmetic and copies ran while one was open for 9% of the time, Pallas kernels for 22%

profile of v2, /device:TPU:0, one launch (start us, length us, event | category | flops | bytes accessed | tf_op | source)
XLA Modules:
  0.0 253.1 jit_solution(10183718327713573374)
XLA Ops:
  6.5 0.0 copy-start.3
  6.5 0.0 all-gather.4.cloned.1.call-start
  6.5 1.5 copy.30
  8.1 1.2 copy.31
  9.2 0.0 copy-done.3
  9.2 0.3 copy.32
  9.6 1.2 copy.33
  10.8 53.6 %chunk.1 = (f32[128,512]{1,0:T(8,128)}, f32[128,512]{1,0:T(8,128)}, bf16[8,64,128]{2,1,0:T(8,128)(2,1)}, bf16[4,128,704]{2,1,0:T(8,128)(2,1)}, bf16[4,128,704]{2...) custom-call(bf16[128,512]{1,0:T(8,128)(2,1)} %r_ref.3, bf16[128,512]{1,0:T(8,128)(2,1)} %k_ref.3, bf16[128,512]{1,0:T(8,128)(2,1)} %v_ref.3, ...), custom_call_target="tpu_custom_call" | custom-call | flops 1600000000 | bytes 1441792 | tf_op jit(solution)/shard_map/chunk/pallas_call | solution.py:173
  64.3 0.0 copy-start.2
  64.3 2.4 copy.34
  66.7 0.0 all-gather.4.cloned.1.call-update
  66.7 0.0 all-gather.8.cloned.1.call-start
  66.8 0.7 all-gather.8.cloned.1.call-update
  67.5 0.0 all-gather.6.cloned.1.call-start
  67.5 0.0 copy-done.2
  67.5 1.1 copy.38
  68.7 0.0 all-gather.6.cloned.1.call-update
  68.7 0.0 reduce-scatter.2.cloned.1.call-start
  68.7 55.7 %finish.1 = (bf16[4,2,64,2048]{3,2,1,0:T(8,128)(2,1)}, f32[64,2048]{1,0:T(8,128)}) custom-call(bf16[8,64,128]{2,1,0:T(8,128)(2,1)} %get-tuple-element.13.m_ref, f32[128,512]{1,0:T(8,128)} %get-tuple-element.14.q_ref, f32[128,512]{1,0:T(8,128)} %get-tuple-element.15.o_ref, bf16[128,512]{1,0:T(8,128)(2,1)} %r_ref.3, bf16[128,512]{1,0:T(8,128)(2,1)} %k_ref.3, ...), custom_call_target="tpu_custom_call" | custom-call | flops 20000000000 | bytes 4000000 | tf_op jit(solution)/shard_map/finish/pallas_call | solution.py:318
  124.5 0.0 all-gather.4.cloned.1.call-done
  124.5 4.1 %fusion.9 = bf16[512,704]{0,1:T(8,128)(2,1)S(1)} fusion(bf16[512,2048]{1,0:T(8,128)(2,1)} %bitcast.65, bf16[16,128,704]{1,2,0:T(8,128)(2,1)} %all-gather.4.cloned.1.call-done), kind=kOutput, calls=%fused_computation.17 | convolution fusion | flops 1476755456 | bytes 5701632 | tf_op jit(solution)/shard_map/dot_general | solution.py:368
  128.7 0.2 reshape.38
  128.8 0.0 copy-start
  128.8 0.5 slice.32
  129.3 0.4 copy.41
  129.8 1.7 collective-permute-start
  131.5 0.9 dynamic-slice_reduce_fusion.2
  132.4 25.0 %all-gather.8.cloned.1.call-done = bf16[16,704,128]{2,1,0:T(8,128)(2,1)} async-done(((bf16[4,704,128]{2,1,0:T(8,128)(2,1)}), bf16[16,704,128]{2,1,0:T(8,128)(2,1)}) %all-gather.8.cloned.1.call-update) | async-done | bytes 2883600 | tf_op jit(solution)/shard_map/all_gather | solution.py:361
  157.4 0.0 copy-done
  157.4 4.0 %copy.65 = bf16[1,4,4,704,128]{4,1,2,3,0:T(4,128)(2,1)S(1)} copy(bf16[1,4,4,704,128]{4,3,2,1,0:T(8,128)(2,1)} %bitcast.54) | data formatting | bytes 5767168 | tf_op jit(solution)/shard_map/reshape | solution.py:386
  161.4 3.4 %reshape.42 = bf16[704,2048]{1,0:T(8,128)(2,1)} reshape(bf16[704,1,4,4,128]{4,3,2,0,1:T(4,128)(2,1)S(1)} %bitcast.53) | data formatting | bytes 5767168 | tf_op jit(solution)/shard_map/reshape | solution.py:387
  164.8 0.0 collective-permute-done
  164.8 0.4 copy.37
  165.3 2.4 maximum_convert_fusion
  167.7 0.0 copy-start.1
  167.7 5.3 %divide_multiply_fusion = f32[4,128,704]{1,0,2:T(4,128)} fusion(f32[4,130,704]{1,0,2:T(4,128)S(1)} %maximum_convert_fusion, f32[704]{0:T(1024)S(1)} %get-tuple-element.23, f32[704]{0:T(1024)S(1)} %get-tuple-element.22, f32[704]{0:T(1024)S(1)} %get-tuple-element.21), kind=kLoop, calls=%fused_computation.8 | loop fusion | flops 3244032 | bytes 5775616 | tf_op jit(solution)/shard_map/jit(silu)/mul | solution.py:385
  172.9 28.0 %all-gather.6.cloned.1.call-done = bf16[16,128,704]{1,2,0:T(8,128)(2,1)} async-done(((bf16[4,128,704]{1,2,0:T(8,128)(2,1)}), bf16[16,128,704]{1,2,0:T(8,128)(2,1)}) %all-gather.6.cloned.1.call-update) | async-done | bytes 2883600 | tf_op jit(solution)/shard_map/all_gather | solution.py:360
  200.9 0.0 copy-done.1
  200.9 7.6 %convolution_convert_fusion = bf16[512,2048]{1,0:T(8,128)(2,1)} fusion(bf16[704,2048]{1,0:T(8,128)(2,1)S(1)} %copy-done.1, f32[88,8,4,128]{3,2,1,0:T(4,128)} %bitcast.57, bf16[512,2048]{1,0:T(8,128)(2,1)} %bitcast.66, bf16[16,128,704]{1,2,0:T(8,128)(2,1)} %all-gather.6.cloned.1.call-done), kind=kOutput, calls=%fused_computation | convolution fusion | flops 2955280384 | bytes 11403264 | tf_op jit(solution)/shard_map/dot_general | solution.py:389
  208.6 0.0 copy-start.4
  208.6 0.0 reduce-scatter.2.cloned.1.call-update
  208.6 36.2 %reduce-scatter.2.cloned.1.call-done = bf16[64,2048]{1,0:T(8,128)(2,1)} async-done(((bf16[512,2048]{1,0:T(8,128)(2,1)}), bf16[64,2048]{1,0:T(8,128)(2,1)}) %reduce-scatter.2.cloned.1.call-update) | async-done | bytes 262160 | tf_op jit(solution)/shard_map/reduce_scatter | solution.py:388
  244.8 0.0 copy-done.4
  244.8 1.7 add_convert_fusion
  (1 shorter events, 0.0 us)
Async XLA Ops:
  6.5 2.7 %copy-start.3 = (bf16[128,2816]{1,0:T(8,128)(2,1)S(1)}, bf16[128,2816]{1,0:T(8,128)(2,1)}, u32[]{:S(2)}) copy-start(bf16[128,2816]{1,0:T(8,128)(2,1)} %param.27) | copy-start | bytes 2162692
  6.5 118.0 %all-gather.4.cloned.1.call-start = ((), (), s32[]{:S(2)}) async-start(), calls=%async_computation.1 | async-start | bytes 3604480 | tf_op jit(solution)/shard_map/all_gather | solution.py:359
  64.3 3.2 %copy-start.2 = (bf16[4,128,704]{2,1,0:T(8,128)(2,1)S(1)}, bf16[4,128,704]{2,1,0:T(8,128)(2,1)}, u32[]{:S(2)}) copy-start(bf16[4,128,704]{2,1,0:T(8,128)(2,1)} %get-tuple-element.19) | copy-start | bytes 2162692
  66.7 90.7 %all-gather.8.cloned.1.call-start = ((), (), s32[]{:S(2)}) async-start(), calls=%async_computation.3 | async-start | bytes 3604480 | tf_op jit(solution)/shard_map/all_gather | solution.py:361
  67.5 133.5 %all-gather.6.cloned.1.call-start = ((), (), s32[]{:S(2)}) async-start(), calls=%async_computation.2 | async-start | bytes 3604480 | tf_op jit(solution)/shard_map/all_gather | solution.py:360
  68.7 176.1 %reduce-scatter.2.cloned.1.call-start = ((), (), s32[]{:S(2)}) async-start(), calls=%async_computation.4 | async-start | bytes 2359296 | tf_op jit(solution)/shard_map/reduce_scatter | solution.py:388
  128.8 28.5 %copy-start = (bf16[4,128,704]{1,0,2:T(4,128)(2,1)}, bf16[4,128,704]{1,0,2:T(4,128)(2,1)S(1)}, u32[]{:S(2)}) copy-start(bf16[4,128,704]{1,0,2:T(4,128)(2,1)S(1)} %reshape.38) | copy-start | bytes 2162692
  129.8 35.0 %collective-permute-start = (bf16[4,2,704]{2,0,1:T(4,128)(2,1)S(1)}, bf16[4,2,704]{2,0,1:T(4,128)(2,1)S(1)}, u32[]{:S(2)}, u32[]{:S(2)}) collective-permute-start(bf16[4,2,704]{2,0,1:T(4,128)(2,1)S(1)} %copy.41), channel_id=1, source_target_pairs={{0,2},{2,4},{4,6},{6,0},{1,3},{3,5},{5,7},{7,1},{8,10},{10,12},{12... | collective-permute-start | bytes 33800 | tf_op jit(solution)/shard_map/ppermute | solution.py:372
  167.7 33.3 %copy-start.1 = (bf16[704,2048]{1,0:T(8,128)(2,1)S(1)}, bf16[704,2048]{1,0:T(8,128)(2,1)}, u32[]{:S(2)}) copy-start(bf16[704,2048]{1,0:T(8,128)(2,1)} %reshape.42) | copy-start | bytes 8650756
  208.6 36.3 %copy-start.4 = (f32[64,2048]{1,0:T(8,128)S(1)}, f32[64,2048]{1,0:T(8,128)}, u32[]{:S(2)}) copy-start(f32[64,2048]{1,0:T(8,128)} %get-tuple-element.16) | copy-start | bytes 1572868
Sparse Core Ops, SparseCore 0:
  66.8 46.9 all-gather.3
  115.6 41.6 all-gather.7
  159.2 41.6 all-gather.5
  208.7 36.0 reduce-scatter.1

commit v3 on v2

--- a/solution.py
+++ b/solution.py
@@ -40,20 +40,20 @@
 def peers(kinds):
     found = []
     for kind in kinds:
-        if kind[0] == "oa":
-            found += outer_peers()[0]
+        if kind[0] in ("oa", "ob"):
+            found += joint_peers(kind[0][1])[0]
         else:
             found += [{kind[0]: to} for to, _ in others(kind[0])]
     return found
 
 
-def outer_peers():
-    count, size = lax.axis_size("o") * lax.axis_size("a"), lax.axis_size("a")
-    me = lax.axis_index("o") * size + lax.axis_index("a")
+def joint_peers(inner):
+    count, size = lax.axis_size("o") * lax.axis_size(inner), lax.axis_size(inner)
+    me = lax.axis_index("o") * size + lax.axis_index(inner)
     to, come = [], []
     for d in range(1, count):
         there = lax.rem(me + d, count)
-        to.append({"o": there // size, "a": lax.rem(there, size)})
+        to.append({"o": there // size, inner: lax.rem(there, size)})
         come.append(lax.rem(me + count - d, count))
     return to, come, me
 
@@ -72,30 +72,48 @@
     )
 
 
-def exchange(sources, targets, sends, recvs, local, begin):
+def exchange(sources, targets, sends, recvs, local, step):
     me = lax.axis_index("a")
-    for n, (src, dst) in enumerate(zip(sources, targets)):
+    mine = joint_peers("b")[2]
+    for n, (src, whole) in enumerate(zip(sources, targets)):
+        dst = whole.at[mine]
         own = pltpu.make_async_copy(src.at[me], dst.at[me], local.at[n])
-        if begin:
+        if step == "start":
             own.start()
         for d, (to, come) in enumerate(others("a")):
             out = remote(src.at[to], dst.at[me], sends.at[n, d], recvs.at[n, me], {"a": to})
-            if begin:
+            if step == "start":
                 out.start()
-            else:
+            elif step == n:
                 out.wait_send()
                 remote(src.at[to], dst.at[come], sends.at[n, d], recvs.at[n, come], {"a": to}).wait_recv()
-        if not begin:
+        if step == n:
             own.wait()
 
 
-def chunk_kernel(r_ref, k_ref, v_ref, x_ref, l_ref, gate, up, down, q_ref, o_ref, m_ref, gate_out, up_out, down_out, sends, recvs, local):
+def spread_out(whole, sends, recvs, begin):
+    devices, origins, mine = joint_peers("b")
+    for d, (device, come) in enumerate(zip(devices, origins)):
+        out = remote(whole.at[mine], whole.at[mine], sends.at[d], recvs.at[mine], device)
+        if begin:
+            out.start()
+        else:
+            out.wait_send()
+            remote(whole.at[mine], whole.at[come], sends.at[d], recvs.at[come], device).wait_recv()
+
+
+def chunk_kernel(r_ref, k_ref, v_ref, x_ref, l_ref, gate, up, down, q_ref, o_ref, m_ref, gate_out, up_out, down_out, sends, recvs, local, wide_s, wide_r):
     swap = functools.partial(exchange, (gate, up, down), (gate_out, up_out, down_out), sends, recvs, local)
 
     @pl.when(pl.program_id(0) == 0)
     def _():
-        greet([("a",)])
-        swap(True)
+        greet([("a",), ("ob",)])
+        swap("start")
+
+    @pl.when(pl.program_id(0) == pl.num_programs(0) - 1)
+    def _():
+        swap(0)
+        spread_out(gate_out, wide_s, wide_r, True)
 
     tokens, lanes = r_ref.shape
     row = lax.broadcasted_iota(jnp.int32, (tokens, tokens), 0)
@@ -160,7 +178,9 @@
 
     @pl.when(pl.program_id(0) == pl.num_programs(0) - 1)
     def _():
-        swap(False)
+        swap(1)
+        swap(2)
+        spread_out(gate_out, wide_s, wide_r, False)
 
 
 def chunk(r, k, v, x, l, gate, up, down):
@@ -168,6 +188,7 @@
     pair = 2 * WIDTH
     heads = channels // WIDTH
     size = gate.shape[0]
+    side = lax.axis_size("o") * lax.axis_size("b")
     block = pl.BlockSpec((tokens, pair), lambda i: (0, i))
     hbm = pl.BlockSpec(memory_space=pltpu.HBM)
     return pl.pallas_call(
@@ -178,13 +199,15 @@
             jax.ShapeDtypeStruct((tokens, channels), f32),
             jax.ShapeDtypeStruct((heads, WIDTH, pair), bf16),
         )
-        + tuple(jax.ShapeDtypeStruct(w.shape, bf16) for w in (gate, up, down)),
+        + tuple(jax.ShapeDtypeStruct((side,) + w.shape, bf16) for w in (gate, up, down)),
         in_specs=[block] * 5 + [hbm] * 3,
         out_specs=(block, block, pl.BlockSpec((2, WIDTH, pair), lambda i: (i, 0, 0)), hbm, hbm, hbm),
         scratch_shapes=[
             pltpu.SemaphoreType.DMA((3, size)),
             pltpu.SemaphoreType.DMA((3, size)),
             pltpu.SemaphoreType.DMA((3,)),
+            pltpu.SemaphoreType.DMA((side,)),
+            pltpu.SemaphoreType.DMA((side,)),
         ],
         compiler_params=pltpu.CompilerParams(collective_id=0, has_side_effects=True),
         cost_estimate=pl.CostEstimate(
@@ -195,21 +218,23 @@
 
 
 def finish_kernel(
-    m_ref, q_ref, o_ref, r_ref, k_ref, v_ref, g_ref, e_ref, s_ref, w_ref, skip_ref, gain_ref,
-    rows_ref, res_ref,
-    near, total, far, mixed, partial, parts, near_s, near_r, far_s, far_r, part_s, part_r, row_s, row_r, pass_s,
+    m_ref, q_ref, o_ref, r_ref, k_ref, v_ref, g_ref, e_ref, s_ref, w_ref, skip_ref, gain_ref, up_in, down_in,
+    rows_ref, res_ref, up_ref, down_ref,
+    near, total, far, mixed, partial, parts, near_s, near_r, far_s, far_r, part_s, part_r, row_s, row_r, pass_s, wide_s, wide_r,
 ):
     heads = m_ref.shape[0]
     side, across = lax.axis_size("b"), far.shape[0]
     b, a, t = lax.axis_index("b"), lax.axis_index("a"), lax.axis_index("t")
     wide = lax.axis_size("t")
-    greet([("b",), ("oa",), ("t",)])
+    greet([("ob",), ("oa",), ("t",)])
 
     sent = []
     for d, (to, come) in enumerate(others("b")):
         copy = remote(m_ref, near.at[b], near_s.at[d], near_r.at[b], {"b": to})
         copy.start()
         sent.append(copy)
+    for n, whole in enumerate((up_ref, down_ref)):
+        spread_out(whole, wide_s.at[n], wide_r.at[n], True)
     for to, come in others("b"):
         remote(m_ref, near.at[come], near_s.at[0], near_r.at[come], {"b": to}).wait_recv()
     near[b] = m_ref[...]
@@ -234,7 +259,7 @@
                 )
         total[head] = jnp.concatenate([running[:WIDTH], running[WIDTH:]], axis=1).astype(bf16)
 
-    to_outer, come_outer, outer = outer_peers()
+    to_outer, come_outer, outer = joint_peers("a")
     for d, device in enumerate(to_outer):
         copy = remote(total, far.at[outer], far_s.at[d], far_r.at[outer], device)
         copy.start()
@@ -306,23 +331,30 @@
             remote(theirs, theirs, row_s.at[0], row_r.at[i, come], {"t": to}).wait_recv()
     for copy in sent:
         copy.wait_send()
-
-
-def finish(m, q, o, r, k, v, g, extra, scale, weights, skip, gain):
+    for n, whole in enumerate((up_ref, down_ref)):
+        spread_out(whole, wide_s.at[n], wide_r.at[n], False)
+
+
+def finish(m, q, o, r, k, v, g, extra, scale, weights, skip, gain, up, down):
     tokens, channels = r.shape
     own, model = skip.shape
     side, along, wide = (lax.axis_size(x) for x in ("b", "a", "t"))
     across = lax.axis_size("o") * along
     vmem = pl.BlockSpec(memory_space=pltpu.VMEM)
+    hbm = pl.BlockSpec(memory_space=pltpu.HBM)
+    plane = up.shape[0]
     dma = pltpu.SemaphoreType.DMA
     return pl.pallas_call(
         finish_kernel,
         out_shape=(
             jax.ShapeDtypeStruct((along, wide, own, model), bf16),
             jax.ShapeDtypeStruct((own, model), f32),
+            jax.ShapeDtypeStruct(up.shape, bf16),
+            jax.ShapeDtypeStruct(down.shape, bf16),
         ),
-        in_specs=[vmem] * 12,
-        out_specs=(vmem, vmem),
+        in_specs=[vmem] * 12 + [hbm] * 2,
+        out_specs=(vmem, vmem, hbm, hbm),
+        input_output_aliases={12: 2, 13: 3},
         scratch_shapes=[
             pltpu.VMEM((side,) + m.shape, bf16),
             pltpu.VMEM(m.shape, bf16),
@@ -332,13 +364,14 @@
             pltpu.VMEM((wide, own, model), bf16),
             dma((side,)), dma((side,)), dma((across,)), dma((across,)),
             dma((wide,)), dma((wide,)), dma((along,)), dma((along, wide)), dma((along, wide)),
+            dma((2, plane)), dma((2, plane)),
         ],
         compiler_params=pltpu.CompilerParams(collective_id=1, has_side_effects=True),
         cost_estimate=pl.CostEstimate(
             flops=20_000_000_000, bytes_accessed=4_000_000, transcendentals=0
         ),
         name="finish",
-    )(m, q, o, r, k, v, g, extra[None], scale[None], weights, skip, gain[None])
+    )(m, q, o, r, k, v, g, extra[None], scale[None], weights, skip, gain[None], up, down)
 
 
 def body(
@@ -353,14 +386,11 @@
     def by_owner(w):
         return jnp.moveaxis(w.reshape(piece, along, units), 1, 0)
 
-    q, o, m, gate_part, up_part, down_part = chunk(
+    q, o, m, gate_full, up_part, down_part = chunk(
         r, k, v, x, l, by_owner(gate_w), by_owner(up_w), down_w.reshape(along, units, piece)
     )
-    gate_full = lax.all_gather(gate_part, ("o", "b"), axis=0, tiled=True)
-    up_full = lax.all_gather(up_part, ("o", "b"), axis=0, tiled=True)
-    down_full = lax.all_gather(down_part, ("o", "b"), axis=0, tiled=True)
-    rows, hidden_res = finish(
-        m, q, o, r, k, v, g, extra, scale, exit_weights, skip, gain
+    rows, hidden_res, up_full, down_full = finish(
+        m, q, o, r, k, v, g, extra, scale, exit_weights, skip, gain, up_part, down_part
     )
     rows = rows.reshape(along * tokens, -1)
     model = rows.shape[1]

time: 253 us -> 233 us (0.921)
  waiting for transfers between devices: 89.9 us -> 35.3 us
  Pallas kernels: 109 us -> 147 us
  local copies, waits for them, and re-layouts: 17.6 us -> 14 us
    all_gather x3 -> x0, waiting for transfers between devices: 53 us -> none  [the longest x1 28 us: body(): up_full = lax.all_gather(up_part, ('o', 'b'), axis=0, tiled=True)]
    pallas_call x1, Pallas kernels: 55.7 us -> 88.3 us  [finish(): pl.pallas_call(finish_kernel, out_shape=(jax.ShapeDtypeStruct((along, wid...]
    pallas_call x1, Pallas kernels: 53.6 us -> 59 us  [chunk(): pl.pallas_call(chunk_kernel, grid=(channels // pair,), out_shape=(jax.Sha...]
    reshape x1 -> x0, local copies, waits for them, and re-layouts: 4.04 us -> none  [body(): down_full.reshape(outer, side, along, units, piece)]
    another operation x0 -> x1, local copies, waits for them, and re-layouts: none -> 4.04 us  [body(): down_full = jnp.swapaxes(down_full, 2, 3).reshape(units, model)]
    pallas_call x2 -> x0, local copies, waits for them, and re-layouts: 3.51 us -> none  [chunk(): pl.pallas_call(chunk_kernel, grid=(channels // pair,), out_shape=(jax.Sha...]
  transfers between devices with their start and end apart: 5 -> 2, of which waited for: 3 -> 1; matrix products, arithmetic and copies ran while one was open for 9% -> 4% of each run, Pallas kernels for 22% -> 0%
where the time goes in v3:
time: 233 us
  Pallas kernels  147 us (63%)
  waiting for transfers between devices  35.3 us (15%)
  local copies, waits for them, and re-layouts  14 us (6%)
  between operations  13.5 us (6%)
  matrix products  11.9 us (5%)
  other arithmetic  9.37 us (4%)
    pallas_call x1, Pallas kernels, finish(): pl.pallas_call(finish_kernel, out_shape=(jax.ShapeDtypeStruct((along, wid...  88.3 us
    pallas_call x1, Pallas kernels, chunk(): pl.pallas_call(chunk_kernel, grid=(channels // pair,), out_shape=(jax.Sha...  59 us
    reduce_scatter x1, waiting for transfers between devices, body(): lax.psum_scatter(jnp.dot(hidden, down_full, preferred_element_type=f32).a...  35.3 us
    dot_general x1, matrix products, body(): jnp.dot(hidden, down_full, preferred_element_type=f32).astype(bf16)  7.73 us
    mul x1, other arithmetic, body(): jax.nn.silu(conv_out).reshape(up_out.shape) * up_out.astype(f32)  5.3 us
  transfers between devices with their start and end apart: 2, of which 1 were waited for; matrix products, arithmetic and copies ran while one was open for 4% of the time, Pallas kernels for 0%

profile of v3, /device:TPU:0, one launch (start us, length us, event | category | flops | bytes accessed | tf_op | source)
XLA Modules:
  0.0 233.1 jit_solution(17441878834109813637)
XLA Ops:
  6.5 0.0 copy-start.2
  6.5 0.0 reduce-scatter.2.cloned.1.call-start
  6.5 1.5 copy.23
  8.1 1.2 copy.24
  9.2 0.0 copy-done.2
  9.2 0.3 copy.25
  9.6 1.2 copy.26
  10.8 59.0 %chunk.1 = (f32[128,512]{1,0:T(8,128)}, f32[128,512]{1,0:T(8,128)}, bf16[8,64,128]{2,1,0:T(8,128)(2,1)}, bf16[4,4,128,704]{3,2,1,0:T(8,128)(2,1)}, bf16[4,4,128,...) custom-call(bf16[128,512]{1,0:T(8,128)(2,1)} %r_ref.3, bf16[128,512]{1,0:T(8,128)(2,1)} %k_ref.3, ...), custom_call_target="tpu_custom_call" | custom-call | flops 1600000000 | bytes 1441792 | tf_op jit(solution)/shard_map/chunk/pallas_call | solution.py:194
  69.7 88.3 %finish.1 = (bf16[4,2,64,2048]{3,2,1,0:T(8,128)(2,1)}, f32[64,2048]{1,0:T(8,128)}, bf16[4,4,128,704]{3,2,1,0:T(8,128)(2,1)}, bf16[4,4,704,128]{3,2,1,0:T(8,128)(2,1)}) custom-call(bf16[8,64,128]{2,1,0:T(8,128)(2,1)} %get-tuple-element.15.m_ref, f32[128,512]{1,0:T(8,128)} %get-tuple-element.16.q_ref, ...), custom_call_target="tpu_custom_call", output_to_operand_aliasing={{2}: (12, {}), {3}: (13, {})} | custom-call | flops 20000000000 | bytes 4000000 | tf_op jit(solution)/shard_map/finish/pallas_call | solution.py:347
  158.1 4.2 %convolution_convert_fusion.2 = bf16[512,704]{0,1:T(8,128)(2,1)S(1)} fusion(bf16[512,2048]{1,0:T(8,128)(2,1)} %bitcast.46, bf16[2048,704]{1,0:T(8,128)(2,1)} %bitcast.44), kind=kOutput, calls=%fused_computation.11 | convolution fusion | flops 1476755456 | bytes 5701632 | tf_op jit(solution)/shard_map/dot_general | solution.py:398
  162.3 0.2 reshape.38
  162.5 0.0 copy-start
  162.5 0.5 slice.32
  163.0 0.4 copy.30
  163.4 1.6 collective-permute-start
  165.0 0.0 copy-done
  165.0 4.0 %copy.29 = bf16[704,1,4,4,128]{4,3,2,0,1:T(4,128)(2,1)S(1)} copy(bf16[704,1,4,4,128]{4,0,2,3,1:T(8,128)(2,1)} %bitcast.33) | data formatting | bytes 5767168 | tf_op jit(solution)/shard_map/transpose;transpose | solution.py:417
  169.1 3.3 %reshape.42 = bf16[704,2048]{1,0:T(8,128)(2,1)} reshape(bf16[704,1,4,4,128]{4,3,2,0,1:T(4,128)(2,1)S(1)} %copy.29) | data formatting | bytes 5767168 | tf_op jit(solution)/shard_map/reshape | solution.py:417
  172.4 0.9 dynamic-slice_reduce_fusion.2
  173.4 0.0 collective-permute-done
  173.4 0.4 copy.28
  173.8 2.3 %maximum_convert_fusion = f32[4,130,704]{1,0,2:T(4,128)S(1)} fusion(bf16[4,128,704]{1,0,2:T(4,128)(2,1)} %copy-done, bf16[4,2,704]{1,0,2:T(4,128)(2,1)S(1)} %copy.28), kind=kLoop, calls=%fused_computation.9 | loop fusion | flops 1464320 | bytes 2196480 | tf_op jit(solution)/shard_map/convert_element_type | solution.py:411
  176.2 0.0 copy-start.1
  176.2 5.3 %divide_multiply_fusion = f32[4,128,704]{1,0,2:T(4,128)} fusion(f32[4,130,704]{1,0,2:T(4,128)S(1)} %maximum_convert_fusion, f32[704]{0:T(1024)S(1)} %get-tuple-element.27, f32[704]{0:T(1024)S(1)} %get-tuple-element.26, f32[704]{0:T(1024)S(1)} %get-tuple-element.25), kind=kLoop, calls=%fused_computation.1 | loop fusion | flops 3244032 | bytes 5775616 | tf_op jit(solution)/shard_map/jit(silu)/mul | solution.py:415
  181.5 0.0 copy-done.1
  181.5 7.7 %convolution_convert_fusion = bf16[512,2048]{1,0:T(8,128)(2,1)} fusion(bf16[704,2048]{1,0:T(8,128)(2,1)S(1)} %copy-done.1, f32[88,8,4,128]{3,2,1,0:T(4,128)} %bitcast.36, bf16[512,2048]{1,0:T(8,128)(2,1)} %bitcast.47, bf16[2048,704]{1,0:T(8,128)(2,1)} %bitcast.45), kind=kOutput, calls=%fused_computation | convolution fusion | flops 2955280384 | bytes 11403264 | tf_op jit(solution)/shard_map/dot_general | solution.py:419
  189.2 0.0 copy-start.3
  189.2 0.0 reduce-scatter.2.cloned.1.call-update
  189.3 35.3 %reduce-scatter.2.cloned.1.call-done = bf16[64,2048]{1,0:T(8,128)(2,1)} async-done(((bf16[512,2048]{1,0:T(8,128)(2,1)}), bf16[64,2048]{1,0:T(8,128)(2,1)}) %reduce-scatter.2.cloned.1.call-update) | async-done | bytes 262160 | tf_op jit(solution)/shard_map/reduce_scatter | solution.py:418
  224.6 0.0 copy-done.3
  224.6 1.7 add_convert_fusion
  (1 shorter events, 0.0 us)
Async XLA Ops:
  6.5 2.7 %copy-start.2 = (bf16[128,2816]{1,0:T(8,128)(2,1)S(1)}, bf16[128,2816]{1,0:T(8,128)(2,1)}, u32[]{:S(2)}) copy-start(bf16[128,2816]{1,0:T(8,128)(2,1)} %param.27) | copy-start | bytes 2162692
  6.5 218.0 %reduce-scatter.2.cloned.1.call-start = ((), (), s32[]{:S(2)}) async-start(), calls=%async_computation.1 | async-start | bytes 2359296 | tf_op jit(solution)/shard_map/reduce_scatter | solution.py:418
  162.5 2.6 %copy-start = (bf16[4,128,704]{1,0,2:T(4,128)(2,1)}, bf16[4,128,704]{1,0,2:T(4,128)(2,1)S(1)}, u32[]{:S(2)}) copy-start(bf16[4,128,704]{1,0,2:T(4,128)(2,1)S(1)} %reshape.38) | copy-start | bytes 2162692
  163.4 10.0 %collective-permute-start = (bf16[4,2,704]{2,0,1:T(4,128)(2,1)S(1)}, bf16[4,2,704]{2,0,1:T(4,128)(2,1)S(1)}, u32[]{:S(2)}, u32[]{:S(2)}) collective-permute-start(bf16[4,2,704]{2,0,1:T(4,128)(2,1)S(1)} %copy.30), channel_id=1, source_target_pairs={{0,2},{2,4},{4,6},{6,0},{1,3},{3,5},{5,7},{7,1},{8,10},{10,12},{12... | collective-permute-start | bytes 33800 | tf_op jit(solution)/shard_map/ppermute | solution.py:402
  176.2 5.3 %copy-start.1 = (bf16[704,2048]{1,0:T(8,128)(2,1)S(1)}, bf16[704,2048]{1,0:T(8,128)(2,1)}, u32[]{:S(2)}) copy-start(bf16[704,2048]{1,0:T(8,128)(2,1)} %reshape.42) | copy-start | bytes 8650756
  189.2 35.3 %copy-start.3 = (f32[64,2048]{1,0:T(8,128)S(1)}, f32[64,2048]{1,0:T(8,128)}, u32[]{:S(2)}) copy-start(f32[64,2048]{1,0:T(8,128)} %get-tuple-element.20) | copy-start | bytes 1572868
Sparse Core Ops, SparseCore 0:
  189.4 35.1 reduce-scatter.1
